TPU v7x, 128 devices: a whole 4x4x4 slice. The times are simulated.
128 devices in a mesh: sp: 16 (over z, x), fs: 4 (over y), tp: 2 (over core).
Axes of the slice: x: 4, y: 4, z: 4, core: 2. Of those that a mesh axis runs over, the one named last changes fastest.
Arguments:
- tokens: bfloat16 [4, 16384, 2048], P('fs', ('sp', 'tp')), may hold values from -6 to 6
- norm_gain: bfloat16 [2048], replicated, may hold values from 0.099609375 to 1.8984375
- w_query: bfloat16 [2048, 1024], P(None, 'tp'), may hold values from -0.125 to 0.125
- w_key: bfloat16 [2048, 1024], P(None, 'tp'), may hold values from -0.125 to 0.125
- w_value: bfloat16 [2048, 1024], P(None, 'tp'), may hold values from -0.125 to 0.125
- w_outgate: bfloat16 [2048, 1024], P(None, 'tp'), may hold values from -0.125 to 0.125
- w_gatein: bfloat16 [2048, 1024], P(None, 'tp'), may hold values from -0.125 to 0.125
- w_gateout: bfloat16 [2048, 1024], P(None, 'tp'), may hold values from -0.125 to 0.125
- w_convin: bfloat16 [2048, 1024], P(None, 'tp'), may hold values from -0.125 to 0.125
- w_igate: bfloat16 [2048, 8], replicated, may hold values from -0.125 to 0.125
- w_fgate: bfloat16 [2048, 8], replicated, may hold values from -0.125 to 0.125
- input_bias: float32 [8], replicated, may hold values from -1 to 101
- forget_bias: float32 [8], replicated
- forget_extra: float32 [4, 16384, 8], P('fs', 'sp', 'tp'), may hold values from -0.7 to 0
- init_memory: float32 [4, 8, 128, 128], P('fs', 'tp'), may hold values from -112 to 112
- head_gain: bfloat16 [1024], replicated, may hold values from 0.099609375 to 1.8984375
- conv_taps: bfloat16 [3, 1024], replicated, may hold values from -3.5 to 3.5
- out_memory: bfloat16 [1024, 2048], P('tp'), may hold values from -0.125 to 0.125
- out_conv: bfloat16 [1024, 2048], P('tp'), may hold values from -0.125 to 0.125
Outputs:
- layer_out: bfloat16 [4, 16384, 2048], P('fs', ('sp', 'tp'))
All inputs are finite; a program needn't handle non-finite values.
Results may differ from a plain program's by a relative error of at most 0.017.
Values may be sent and summed in bfloat16 or wider, within the bound.
A program may use at most 128 MiB of HBM per device.

v0:
```python
import jax
import jax.numpy as jnp
from jax import lax
from jax.sharding import Mesh
from jax.sharding import PartitionSpec as P

BLOCK = 128
SP = ("sp_0", "sp_1")
SP_TP = ("sp_0", "sp_1", "tp")


EPSILON = 1e-06
LOWEST_LOG = -1e30


def shifted(block, axis, distance):
    devices = range(lax.axis_size(axis))
    route = [(i - distance, i) for i in devices if i - distance in devices]
    return lax.ppermute(block, axis, route)


def nothing_yet(value, identity):
    return jax.tree.map(
        lambda part, zero: jnp.zeros_like(part) + jnp.asarray(zero, part.dtype), value, identity
    )


def prefix_by_axis(value, axes, combine, identity):
    before = start = nothing_yet(value, identity)
    subtotal = value
    for axis in reversed(axes):
        size, mine = (lax.axis_size(axis), lax.axis_index(axis))
        pieces = jax.tree.map(lambda part: lax.all_gather(part, axis), subtotal)
        inside, subtotal = (start, start)
        for k in range(size):
            passed = k < mine
            subtotal = combine(subtotal, jax.tree.map(lambda part: part[k], pieces))
            inside = jax.tree.map(lambda new, old: jnp.where(passed, new, old), subtotal, inside)
        before = combine(inside, before)
    return before


def in_blocks(value, dim, size):
    before, after = (value.shape[:dim], value.shape[dim + 1 :])
    return jnp.moveaxis(value.reshape(*before, size, -1, *after), dim, 0)


def sum_at_owner(value, axis, dim):
    size = lax.axis_size(axis)
    blocks = lax.all_to_all(in_blocks(value, dim, size), axis, 0, 0, tiled=True)
    return jnp.sum(blocks.astype(jnp.float32), axis=0)


def compose(memory_pair, segment):
    memory, log_scale = memory_pair
    span_total, seg_memory, seg_scale = segment
    merged = jnp.maximum(span_total + log_scale, seg_scale)
    kept_share = jnp.exp(span_total + log_scale - merged)
    added_share = jnp.exp(seg_scale - merged)
    return (
        kept_share[..., None, None] * memory + added_share[..., None, None] * seg_memory,
        merged,
    )


def combine(earlier, later_part):
    memory, log_scale = compose((earlier[1], earlier[2]), later_part)
    return (earlier[0] + later_part[0], memory, log_scale)


def local(
    tokens,
    norm_gain,
    w_query,
    w_key,
    w_value,
    w_outgate,
    w_gatein,
    w_gateout,
    w_convin,
    w_igate,
    w_fgate,
    input_bias,
    forget_bias,
    forget_extra,
    init_memory,
    head_gain,
    conv_taps,
    out_memory,
    out_conv,
):
    local_heads = init_memory.shape[1]
    head_dim = init_memory.shape[-1]
    width_local = w_query.shape[1]
    key_factor = head_dim ** (-0.5)
    part_index = lax.axis_index("tp")
    own_rows = tokens[0].astype(jnp.float32)
    normed = own_rows * lax.rsqrt(jnp.mean(own_rows * own_rows, axis=-1, keepdims=True) + EPSILON)
    normed = (normed * norm_gain.astype(jnp.float32)).astype(jnp.bfloat16)
    normed_all = lax.all_gather(normed, "tp", axis=0, tiled=True)

    def project(weight):
        return jnp.dot(normed_all, weight, preferred_element_type=jnp.float32).astype(jnp.bfloat16)

    queries = project(w_query)
    key_rows = project(w_key)
    value_rows = project(w_value)
    out_gate = project(w_outgate)
    gate_in = project(w_gatein)
    gate_out = project(w_gateout)
    conv_input = project(w_convin)
    conv_product = (gate_in.astype(jnp.float32) * conv_input.astype(jnp.float32)).astype(
        jnp.bfloat16
    )
    token_count = normed_all.shape[0]
    tap_count = conv_taps.shape[0]
    rim_rows = shifted(conv_product[token_count - tap_count + 1 :], SP, 1)
    head_start = part_index * local_heads
    gate_weights = jnp.concatenate(
        [
            lax.dynamic_slice_in_dim(w_igate, head_start, local_heads, 1),
            lax.dynamic_slice_in_dim(w_fgate, head_start, local_heads, 1),
        ],
        axis=1,
    )
    gate_pre = jnp.dot(normed_all, gate_weights, preferred_element_type=jnp.float32)
    input_pre = gate_pre[:, :local_heads] + lax.dynamic_slice_in_dim(
        input_bias, head_start, local_heads
    )
    forget_pre = gate_pre[:, local_heads:] + lax.dynamic_slice_in_dim(
        forget_bias, head_start, local_heads
    )
    log_forget = jax.nn.log_sigmoid(forget_pre) + forget_extra[0]
    nblocks = token_count // BLOCK
    block_shape = (nblocks, BLOCK, local_heads, head_dim)
    query_blocks = queries.reshape(block_shape)
    key_blocks = key_rows.reshape(block_shape)
    value_blocks = value_rows.reshape(block_shape)
    gate_in_blocks = jnp.swapaxes(input_pre.reshape(nblocks, BLOCK, local_heads), 1, 2)
    forget_blocks = jnp.swapaxes(log_forget.reshape(nblocks, BLOCK, local_heads), 1, 2)
    cumulative = jnp.cumsum(forget_blocks, axis=-1)
    block_total = cumulative[..., -1]
    exponent = block_total[..., None] - cumulative + gate_in_blocks
    block_top = jnp.max(exponent, axis=-1)
    key_weights = jnp.swapaxes(jnp.exp(exponent - block_top[..., None]), 1, 2)[..., None]
    weighted_keys = (key_weights * key_blocks.astype(jnp.float32) * key_factor).astype(jnp.bfloat16)
    block_terms = jnp.einsum(
        "bshd,bshe->bhde", weighted_keys, value_blocks, preferred_element_type=jnp.float32
    )
    identity = (
        jnp.zeros((local_heads,), jnp.float32),
        jnp.zeros((local_heads, head_dim, head_dim), jnp.float32),
        jnp.full((local_heads,), LOWEST_LOG, jnp.float32),
    )

    def block_step(running, element):
        return (combine(running, element), running)

    segment, prefixes = lax.scan(block_step, identity, (block_total, block_terms, block_top))
    start_pair = (init_memory[0], jnp.zeros((local_heads,), jnp.float32))
    earlier = prefix_by_axis(segment, SP, combine, identity)
    incoming = compose(start_pair, earlier)
    starts_memory, starts_scale = compose(incoming, prefixes)
    row_index = lax.broadcasted_iota(jnp.int32, (BLOCK, BLOCK), 0)
    col_index = lax.broadcasted_iota(jnp.int32, (BLOCK, BLOCK), 1)
    pair_log = cumulative[..., :, None] - cumulative[..., None, :] + gate_in_blocks[..., None, :]
    pair_log = jnp.where(col_index <= row_index, pair_log, -jnp.inf)
    carried_log = cumulative + starts_scale[..., None]
    row_top = jnp.maximum(carried_log, jnp.max(pair_log, axis=-1))
    scores = (
        jnp.einsum("bthd,bshd->bhts", query_blocks, key_blocks, preferred_element_type=jnp.float32)
        * key_factor
    )
    weighted = (jnp.exp(pair_log - row_top[..., None]) * scores).astype(jnp.bfloat16)
    carried = jnp.einsum("bthd,bhde->bthe", query_blocks.astype(jnp.float32), starts_memory)
    inter_weight = jnp.swapaxes(jnp.exp(carried_log - row_top), 1, 2)[..., None]
    readout = inter_weight * carried + jnp.einsum(
        "bhts,bshe->bthe", weighted, value_blocks, preferred_element_type=jnp.float32
    )
    normalized = readout * lax.rsqrt(jnp.mean(readout * readout, axis=-1, keepdims=True) + EPSILON)
    gain_local = lax.dynamic_slice_in_dim(head_gain, part_index * width_local, width_local).astype(
        jnp.float32
    )
    memory_out = (
        normalized.reshape(token_count, width_local)
        * gain_local
        * jax.nn.sigmoid(out_gate.astype(jnp.float32))
    )
    memory_out = memory_out.astype(jnp.bfloat16)
    taps_local = lax.dynamic_slice_in_dim(
        conv_taps, part_index * width_local, width_local, 1
    ).astype(jnp.float32)
    padded = jnp.concatenate([rim_rows, conv_product], axis=0).astype(jnp.float32)
    mixed_conv = padded[0:token_count] * taps_local[0]
    for tap_index in range(1, tap_count):
        mixed_conv = (
            mixed_conv + padded[tap_index : tap_index + token_count] * taps_local[tap_index]
        )
    conv_out = (gate_out.astype(jnp.float32) * mixed_conv).astype(jnp.bfloat16)
    layer_rows = sum_at_owner(
        (
            jnp.dot(memory_out, out_memory, preferred_element_type=jnp.float32)
            + jnp.dot(conv_out, out_conv, preferred_element_type=jnp.float32)
        ).astype(jnp.bfloat16),
        "tp",
        0,
    )
    return layer_rows.astype(jnp.bfloat16)[None]


def solution(mesh):
    finer = Mesh(
        mesh.devices.reshape(4, 4, mesh.shape["fs"], mesh.shape["tp"]), ("sp_0", "sp_1", "fs", "tp")
    )
    return jax.shard_map(
        local,
        mesh=finer,
        in_specs=(
            P("fs", SP_TP, None),
            P(),
            P(None, "tp"),
            P(None, "tp"),
            P(None, "tp"),
            P(None, "tp"),
            P(None, "tp"),
            P(None, "tp"),
            P(None, "tp"),
            P(),
            P(),
            P(),
            P(),
            P("fs", SP, "tp"),
            P("fs", "tp", None, None),
            P(),
            P(),
            P("tp", None),
            P("tp", None),
        ),
        out_specs=P("fs", SP_TP, None),
        check_vma=False,
    )
```

profile of v0, /device:TPU:1, one launch (start us, length us, event | category | flops | bytes accessed | tf_op | source)
XLA Modules:
  0.0 203.0 jit_solution(16010630909655677404)
XLA Ops:
  6.5 2.2 %fusion.8 = f32[512]{0:T(512)S(1)} fusion(bf16[1,512,2048]{2,1,0:T(8,128)(2,1)} %param.21), kind=kLoop, calls=%fused_computation.19 | loop fusion | flops 3145216 | bytes 2099200 | tf_op jit(solution)/shard_map/reduce_sum | solution.py:98
  13.0 18.0 %all-gather.9.cloned.1.call-done = bf16[1024,2048]{1,0:T(8,128)(2,1)} async-done(((bf16[512,2048]{1,0:T(8,128)(2,1)}), bf16[1024,2048]{1,0:T(8,128)(2,1)}) %all-gather.9.cloned.1.call-update) | async-done | bytes 4194320 | tf_op jit(solution)/shard_map/all_gather | solution.py:100
  31.0 3.4 %fusion.60 = f32[1024,8]{0,1:T(8,128)S(1)} fusion(bf16[1024,2048]{1,0:T(8,128)(2,1)} %all-gather.9.cloned.1.call-done, bf16[2048,4]{0,1:T(4,128)(2,1)S(1)} %get-tuple-element.203, bf16[2048,4]{0,1:T(4,128)(2,1)S(1)} %get-tuple-element.204), kind=kOutput, calls=%fused_computation.98 | convolution fusion | flops 33619968 | bytes 4259840 | tf_op jit(solution)/shard_map/dot_general | solution.py:126
  36.3 5.3 %convolution_convert_fusion = bf16[1024,512]{1,0:T(8,128)(2,1)S(1)} fusion(bf16[1024,2048]{1,0:T(8,128)(2,1)} %all-gather.9.cloned.1.call-done, bf16[2048,512]{1,0:T(8,128)(2,1)} %param.29), kind=kOutput, calls=%fused_computation.45 | convolution fusion | flops 2148007936 | bytes 7340032 | tf_op jit(solution)/shard_map/dot_general | solution.py:103
  41.6 2.3 %multiply_convert_fusion = bf16[1024,512]{1,0:T(8,128)(2,1)S(1)} fusion(bf16[1024,512]{1,0:T(8,128)(2,1)S(1)} %convolution_convert_fusion, bf16[1024,2048]{1,0:T(8,128)(2,1)S(1)} %copy-done.3, bf16[2048,512]{1,0:T(8,128)(2,1)S(1)} %copy-done.29), kind=kOutput, calls=%fused_computation.34 | convolution fusion | flops 2150105088 | bytes 8388608 | tf_op jit(solution)/shard_map/dot_general | solution.py:103
  44.0 3.2 %collective-permute-start = (bf16[2,512]{1,0:T(2,128)(2,1)S(1)}, bf16[2,512]{1,0:T(2,128)(2,1)S(1)}, u32[]{:S(2)}, u32[]{:S(2)}) collective-permute-start(bf16[2,512]{1,0:T(2,128)(2,1)S(1)} %slice.175), channel_id=1, source_target_pairs={{0,8},{8,16},{16,24},{24,32},{32,40},{40,48},{48,56},{56,64},{64,7... | collective-permute-start | bytes 6152 | tf_op jit(solution)/shard_map/ppermute | solution.py:19
  47.2 3.3 %convolution_convert_fusion.5 = bf16[1024,512]{1,0:T(8,128)(2,1)} fusion(bf16[1024,2048]{1,0:T(8,128)(2,1)S(1)} %copy-done.3, bf16[2048,512]{1,0:T(8,128)(2,1)S(1)} %copy-done.30), kind=kOutput, calls=%fused_computation.50 | convolution fusion | flops 2148007936 | bytes 7340032 | tf_op jit(solution)/shard_map/dot_general | solution.py:103
  53.2 6.2 %convolution_convert_fusion.6 = bf16[1024,512]{1,0:T(8,128)(2,1)} fusion(bf16[1024,2048]{1,0:T(8,128)(2,1)} %all-gather.9.cloned.1.call-done, bf16[2048,512]{1,0:T(8,128)(2,1)} %param.24), kind=kOutput, calls=%fused_computation.51 | convolution fusion | flops 2148007936 | bytes 7340032 | tf_op jit(solution)/shard_map/dot_general | solution.py:103
  62.0 3.7 %fusion.25 = f32[8,4,128,128]{3,2,1,0:T(8,128)} fusion(bf16[8,128,4,128]{1,3,2,0:T(8,128)(2,1)} %copy.66, bf16[8,128,4,128]{1,3,2,0:T(8,128)(2,1)} %copy.50, f32[8,128,4]{1,2,0:T(4,128)S(1)} %copy.49), kind=kOutput, calls=%fused_computation.53 | convolution fusion | flops 136314880 | bytes 4210688 | tf_op jit(solution)/shard_map/bshd,bshe->bhde/dot_general | solution.py:147
  65.7 15.3 %while.21 = (s32[]{:T(128)}, f32[4]{0:T(128)S(1)}, f32[4,128,128]{2,1,0:T(8,128)S(1)}, f32[4]{0:T(128)S(1)}, f32[8,4]{1,0:T(8,128)S(1)}, /*index=5*/f32[8,4,128,...) while((s32[]{:T(128)}, f32[4]{0:T(128)S(1)}, ...), condition=%wide.region_4.5_spmd.clone, body=%wide.region_3.4_spmd.clone.sunk | while | flops 327711 | bytes 1311169 | solution.py:159
  81.8 6.2 %convolution_convert_fusion.4 = bf16[1024,512]{1,0:T(8,128)(2,1)} fusion(bf16[1024,2048]{1,0:T(8,128)(2,1)} %all-gather.9.cloned.1.call-done, bf16[2048,512]{1,0:T(8,128)(2,1)} %param.23), kind=kOutput, calls=%fused_computation.49 | convolution fusion | flops 2148007936 | bytes 7340032 | tf_op jit(solution)/shard_map/dot_general | solution.py:103
  88.4 8.8 %all-reduce.2 = (f32[16]{0:T(128)S(1)}, f32[16]{0:T(128)S(1)}) all-reduce(f32[16]{0:T(128)S(1)} %dynamic-update-slice.1, f32[16]{0:T(128)S(1)} %dynamic-update-slice), channel_id=3, replica_groups=mesh['sp_0'=4,'sp_1'=4,'fs'=4,'tp'=2] {'sp_1'}, use_global_device_ids=true, to_apply=%add.1 | all-reduce | flops 32 | bytes 256
  97.3 6.9 %all-gather.4 = f32[4,1,4]{2,1,0:T(1,128)S(1)} all-gather(f32[1,1,4]{2,1,0:T(1,128)S(1)} %get-tuple-element.167), channel_id=1, replica_groups=mesh['sp_0'=4,'sp_1'=4,'fs'=4,'tp'=2] {'sp_0'}, dimensions={0}, use_global_device_ids=true | all-gather | bytes 80 | tf_op jit(solution)/shard_map/all_gather | solution.py:33
  104.2 6.4 %all-gather.3 = f32[4,1,4]{2,1,0:T(1,128)S(1)} all-gather(f32[1,1,4]{2,1,0:T(1,128)S(1)} %get-tuple-element.200), channel_id=1, replica_groups=mesh['sp_0'=4,'sp_1'=4,'fs'=4,'tp'=2] {'sp_0'}, dimensions={0}, use_global_device_ids=true | all-gather | bytes 80 | tf_op jit(solution)/shard_map/all_gather | solution.py:33
  110.6 2.1 %reshape.741 = bf16[8,128,4,128]{3,2,1,0:T(4,128)(2,1)} reshape(bf16[1024,512]{1,0:T(8,128)(2,1)} %convolution_convert_fusion.4) | data formatting | bytes 2097152 | tf_op jit(solution)/shard_map/reshape | solution.py:136
  117.9 3.9 %fusion.24 = f32[8,4,128,128]{3,2,1,0:T(8,128)} fusion(bf16[8,128,4,128]{1,3,2,0:T(8,128)(2,1)S(1)} %copy-done.5, bf16[8,128,4,128]{1,3,2,0:T(8,128)(2,1)} %copy.50, f32[8,4,128]{2,1,0:T(4,128)S(1)} %copy.63, f32[8,4,128]{2,1,0:T(4,128)S(1)} %copy.57, f32[8,4,128]{2,1,0:T(4,128)S(1)} %copy.55, pred[128,128]{1,0:T(8,128)(4,1)S(1)} %iota_compare_fusion, ...), kind=kOutput, calls=%fused_computation.44 | convolution fusion | flops 272105472 | bytes 5308416 | tf_op jit(solution)/shard_map/bhts,bshe->bthe/dot_general | solution.py:177
  122.6 2.9 %maximum_convert_fusion = f32[1026,512]{1,0:T(8,128)} fusion(bf16[1024,512]{1,0:T(8,128)(2,1)} %copy-done.7, bf16[2,512]{1,0:T(2,128)(2,1)S(1)} %collective-permute-done), kind=kLoop, calls=%fused_computation.52 | loop fusion | flops 2101248 | bytes 3151872 | tf_op jit(solution)/shard_map/convert_element_type | solution.py:193
  125.5 16.2 %all-gather.11.cloned.1.call-done = f32[4,4,128,128]{3,2,1,0:T(8,128)} async-done(((f32[1,4,128,128]{3,2,1,0:T(8,128)}), f32[4,4,128,128]{3,2,1,0:T(8,128)}) %all-gather.11.cloned.1.call-update) | async-done | bytes 1048592 | tf_op jit(solution)/shard_map/all_gather | solution.py:33
  143.7 3.2 %multiply_reduce_fusion = (f32[8,128,4]{1,2,0:T(4,128)S(1)}, f32[8,128,4,128]{1,3,2,0:T(8,128)S(1)}) fusion(f32[8,4,128,128]{3,2,1,0:T(8,128)} %fusion.24, bf16[8,128,4,128]{3,2,1,0:T(4,128)(2,1)S(1)} %copy-done.6, f32[8,4,128,128]{3,2,1,0:T(8,128)} %get-tuple-element.67, f32[8,4]{1,0:T(8,128)S(1)} %subtract_exponential_fusion.2, ...), kind=kOutput, calls=%fused_computation.35 | convolution fusion | flops 137883648 | bytes 7635200 | tf_op jit(solution)/shard_map/bthd,bhde->bthe/dot_general | solution.py:175
  148.4 2.9 %copy.70 = f32[8,128,4,128]{3,2,1,0:T(4,128)} copy(f32[8,128,4,128]{1,3,2,0:T(8,128)} %broadcast_multiply_fusion) | data formatting | bytes 4194304 | tf_op jit(solution)/shard_map/reshape | solution.py:185
  151.3 11.4 %fusion.41 = f32[1024,2048]{1,0:T(8,128)} fusion(bf16[512,2048]{1,0:T(8,128)(2,1)S(1)} %copy-done, f32[128,8,4,128]{3,2,1,0:T(4,128)} %bitcast.379, bf16[1024,2048]{1,0:T(8,128)(2,1)} %all-gather.9.cloned.1.call-done, bf16[2048,512]{1,0:T(8,128)(2,1)} %param.26, f32[512]{0:T(512)S(1)} %dynamic-slice_convert_fusion.1), kind=kOutput, calls=%fused_computation.69 | convolution fusion | flops 4299161600 | bytes 18876416 | tf_op jit(solution)/shard_map/dot_general | solution.py:202
  162.7 14.5 %add_convert_fusion = bf16[1024,2048]{1,0:T(8,128)(2,1)} fusion(f32[1024,2048]{1,0:T(8,128)} %fusion.41, bf16[512,2048]{1,0:T(8,128)(2,1)} %param.39, f32[1026,512]{1,0:T(8,128)} %maximum_convert_fusion, bf16[1024,2048]{1,0:T(8,128)(2,1)} %all-gather.9.cloned.1.call-done, bf16[2048,512]{1,0:T(8,128)(2,1)} %param.28, f32[512]{0:T(512)S(1)} %bitcast.383, ...), kind=kOutput, calls=%fused_computation.16 | convolution fusion | flops 4303880192 | bytes 27269120 | tf_op jit(solution)/shard_map/dot_general | solution.py:203
  177.2 14.2 %all_to_all.5 = bf16[2,512,2048]{2,1,0:T(8,128)(2,1)} all-to-all(bf16[2,512,2048]{2,1,0:T(8,128)(2,1)} %bitcast.378), channel_id=1, replica_groups=mesh['sp_0'=4,'sp_1'=4,'fs'=4,'tp'=2] {'tp'}, dimensions={0} | all-to-all | bytes 8388608 | tf_op jit(solution)/shard_map/all_to_all | solution.py:50
  191.4 5.1 %reduce_sum.32 = bf16[512,2048]{1,0:T(8,128)(2,1)} reduce(bf16[2,512,2048]{2,1,0:T(8,128)(2,1)} %all_to_all.5, bf16[]{:T(256)} %constant.75.clone.1), dimensions={0}, to_apply=%region_7.8 | reduce | flops 1048576 | bytes 6291458 | tf_op jit(solution)/shard_map/reduce_sum | solution.py:51
  (180 shorter events, 36.1 us)
Async XLA Ops:
  6.5 144.8 %copy-start = (bf16[512,2048]{1,0:T(8,128)(2,1)S(1)}, bf16[512,2048]{1,0:T(8,128)(2,1)}, u32[]{:S(2)}) copy-start(bf16[512,2048]{1,0:T(8,128)(2,1)} %param.38) | copy-start | bytes 6291460
  6.5 24.5 %all-gather.9.cloned.1.call-start = ((), (), s32[]{:S(2)}) async-start(), calls=%async_computation.1 | async-start | bytes 6291456 | tf_op jit(solution)/shard_map/all_gather | solution.py:100
  10.9 104.2 %all-gather.13.cloned.1.call-start = ((), (), s32[]{:S(2)}) async-start(), calls=%async_computation.3 | async-start | bytes 1310720 | tf_op jit(solution)/shard_map/all_gather | solution.py:33
  36.3 5.4 %copy-start.3 = (bf16[1024,2048]{1,0:T(8,128)(2,1)S(1)}, bf16[1024,2048]{1,0:T(8,128)(2,1)}, u32[]{:S(2)}) copy-start(bf16[1024,2048]{1,0:T(8,128)(2,1)} %all-gather.9.cloned.1.call-done) | copy-start | bytes 12582916
  41.6 5.6 %copy-start.30 = (bf16[2048,512]{1,0:T(8,128)(2,1)S(1)}, bf16[2048,512]{1,0:T(8,128)(2,1)}, u32[]{:S(2)}) copy-start(bf16[2048,512]{1,0:T(8,128)(2,1)} %param.25) | copy-start | bytes 6291460
  44.0 78.6 %collective-permute-start = (bf16[2,512]{1,0:T(2,128)(2,1)S(1)}, bf16[2,512]{1,0:T(2,128)(2,1)S(1)}, u32[]{:S(2)}, u32[]{:S(2)}) collective-permute-start(bf16[2,512]{1,0:T(2,128)(2,1)S(1)} %slice.175), channel_id=1, source_target_pairs={{0,8},{8,16},{16,24},{24,32},{32,40},{40,48},{48,56},{56,64},{64,7... | collective-permute-start | bytes 6152 | tf_op jit(solution)/shard_map/ppermute | solution.py:19
  81.8 59.9 %all-gather.11.cloned.1.call-start = ((), (), s32[]{:S(2)}) async-start(), calls=%async_computation.2 | async-start | bytes 1310720 | tf_op jit(solution)/shard_map/all_gather | solution.py:33
  88.0 29.9 %copy-start.5 = (bf16[8,128,4,128]{1,3,2,0:T(8,128)(2,1)S(1)}, bf16[8,128,4,128]{1,3,2,0:T(8,128)(2,1)}, u32[]{:S(2)}) copy-start(bf16[8,128,4,128]{1,3,2,0:T(8,128)(2,1)} %copy.66) | copy-start | bytes 3145732
  121.8 19.9 %copy-start.4 = (f32[16,128,128]{2,1,0:T(8,128)S(1)}, f32[16,128,128]{2,1,0:T(8,128)}, u32[]{:S(2)}) copy-start(f32[16,128,128]{2,1,0:T(8,128)} %all-gather.13.cloned.1.call-done) | copy-start | bytes 3145732
  121.8 19.9 %copy-start.8 = (f32[1,4,128,128]{3,2,1,0:T(8,128)S(1)}, f32[1,4,128,128]{3,2,1,0:T(8,128)}, u32[]{:S(2)}) copy-start(f32[1,4,128,128]{3,2,1,0:T(8,128)} %param.35) | copy-start | bytes 786436
  121.8 19.9 %copy-start.14 = (f32[4]{0:T(128)S(1)}, f32[4]{0:T(128)}, u32[]{:S(2)}) copy-start(f32[4]{0:T(128)} %get-tuple-element.157) | copy-start | bytes 52
  121.8 19.9 %copy-start.15 = (f32[4]{0:T(128)S(1)}, f32[4]{0:T(128)}, u32[]{:S(2)}) copy-start(f32[4]{0:T(128)} %get-tuple-element.177) | copy-start | bytes 52
  121.8 19.9 %copy-start.16 = (f32[4]{0:T(128)S(1)}, f32[4]{0:T(128)}, u32[]{:S(2)}) copy-start(f32[4]{0:T(128)} %get-tuple-element.178) | copy-start | bytes 52
  121.8 19.9 %copy-start.17 = (f32[4]{0:T(128)S(1)}, f32[4]{0:T(128)}, u32[]{:S(2)}) copy-start(f32[4]{0:T(128)} %get-tuple-element.179) | copy-start | bytes 52
  121.9 19.9 %copy-start.18 = (f32[4]{0:T(128)S(1)}, f32[4]{0:T(128)}, u32[]{:S(2)}) copy-start(f32[4]{0:T(128)} %get-tuple-element.180) | copy-start | bytes 52
  121.9 19.9 %copy-start.19 = (f32[4]{0:T(128)S(1)}, f32[4]{0:T(128)}, u32[]{:S(2)}) copy-start(f32[4]{0:T(128)} %get-tuple-element.181) | copy-start | bytes 52
  121.9 19.9 %copy-start.20 = (f32[4]{0:T(128)S(1)}, f32[4]{0:T(128)}, u32[]{:S(2)}) copy-start(f32[4]{0:T(128)} %get-tuple-element.182) | copy-start | bytes 52
  121.9 19.9 %copy-start.21 = (f32[4]{0:T(128)S(1)}, f32[4]{0:T(128)}, u32[]{:S(2)}) copy-start(f32[4]{0:T(128)} %get-tuple-element.183) | copy-start | bytes 52
  121.9 19.9 %copy-start.22 = (f32[4]{0:T(128)S(1)}, f32[4]{0:T(128)}, u32[]{:S(2)}) copy-start(f32[4]{0:T(128)} %get-tuple-element.184) | copy-start | bytes 52
  122.5 19.3 %copy-start.23 = (f32[4]{0:T(128)S(1)}, f32[4]{0:T(128)}, u32[]{:S(2)}) copy-start(f32[4]{0:T(128)} %get-tuple-element.187) | copy-start | bytes 52
  122.5 19.3 %copy-start.24 = (f32[4]{0:T(128)S(1)}, f32[4]{0:T(128)}, u32[]{:S(2)}) copy-start(f32[4]{0:T(128)} %get-tuple-element.188) | copy-start | bytes 52
  122.5 19.3 %copy-start.25 = (f32[4]{0:T(128)S(1)}, f32[4]{0:T(128)}, u32[]{:S(2)}) copy-start(f32[4]{0:T(128)} %get-tuple-element.189) | copy-start | bytes 52
  122.5 19.3 %copy-start.26 = (f32[4]{0:T(128)S(1)}, f32[4]{0:T(128)}, u32[]{:S(2)}) copy-start(f32[4]{0:T(128)} %get-tuple-element.198) | copy-start | bytes 52
  122.5 19.3 %copy-start.27 = (f32[4]{0:T(128)S(1)}, f32[4]{0:T(128)}, u32[]{:S(2)}) copy-start(f32[4]{0:T(128)} %get-tuple-element.199) | copy-start | bytes 52
  (14 other events, 30.1 us)
Sparse Core Ops, SparseCore 0:
  11.0 19.9 all-gather.8
  81.9 22.8 all-gather.12
  117.3 24.3 all-gather.10
where the time goes:
time: 204 us; the launch traced here: 203 us
  matrix products  63.3 us (31%)
  other arithmetic  37.2 us (18%)
  blocking collectives  36.3 us (18%)
  waiting for transfers between devices  34.3 us (17%)
  between operations  14.4 us (7%)
  local copies, waits for them, and re-layouts  14 us (7%)
  starting transfers between devices  3.28 us (2%)
    dot_general x5, matrix products, project(): jnp.dot(normed_all, weight, preferred_element_type=jnp.float32)  23.3 us
    all_gather x1, waiting for transfers between devices, local(): normed_all = lax.all_gather(normed, 'tp', axis=0, tiled=True)  18 us
    all_gather x2, waiting for transfers between devices, prefix_by_axis(): pieces = jax.tree.map(lambda part: lax.all_gather(part, axis), subtotal)  16.2 us
    dot_general x1, matrix products, local(): jnp.dot(conv_out, out_conv, preferred_element_type=jnp.float32)  14.5 us
    all_to_all x1, blocking collectives, sum_at_owner(): blocks = lax.all_to_all(in_blocks(value, dim, size), axis, 0, 0, tiled=True)  14.2 us
    all_gather x2, blocking collectives, prefix_by_axis(): pieces = jax.tree.map(lambda part: lax.all_gather(part, axis), subtotal)  13.3 us
    dot_general x1, matrix products, local(): jnp.dot(memory_out, out_memory, preferred_element_type=jnp.float32)  11.4 us
    add x9, other arithmetic, compose(): kept_share[..., None, None] * memory  10.5 us
  transfers between devices with their start and end apart: 4, of which 2 were waited for; matrix products, arithmetic and copies ran while one was open for 27% of the time, Pallas kernels for 0%

commit v1 on v0

v1 whole, which is shorter than its diff:
```python
import functools
import math

import jax
import jax.numpy as jnp
from jax import lax
from jax.experimental import pallas as pl
from jax.experimental.pallas import tpu as pltpu
from jax.sharding import PartitionSpec as P

MESH = pl.DeviceIdType.MESH
F32 = jnp.float32
BF16 = jnp.bfloat16
BLOCK = 128
EPSILON = 1e-06
LOWEST_LOG = -1e30

K_, V_, Q_, OG_, GI_, CI_, GO_ = range(7)
T_BIAS, T_KW, T_ALPHA, T_BETA, T_TOP, T_CARRY = range(6)
L_TOK, L_WIG, L_WFG, L_GAIN, L_FE, L_IB, L_FB, L_TAPS, L_HG, L_OM, L_OC, L_INIT, L_OUT, L_W = (
    0, 1, 2, 3, 4, 5, 6, 7, 8, 9, 10, 11, 12, 16,
)


def kernel(
    n_sp,
    tokens, norm_gain, w_query, w_key, w_value, w_outgate, w_gatein, w_gateout, w_convin,
    w_igate, w_fgate, input_bias, forget_bias, forget_extra, init_memory, head_gain, conv_taps,
    out_memory, out_conv,
    out,
    tok, gain, x, w, wo, wig, wfg, wg, proj, gates, fe, ib, fb, taps, hg, init,
    keys_t, prefix, table, cols, mix, seg, seg_in, scal, scal_in, state_out, state_in,
    rim_in, read, sig, conv, both, part, part_in,
    lsem, tok_s, tok_r, seg_s, seg_r, scal_s, scal_r, st_s, st_r, rim_s, rim_r, out_s, out_r,
):
    own = tokens.shape[1]
    width = tokens.shape[2]
    count = 2 * own
    local_width = w_query.shape[1]
    heads = init_memory.shape[1]
    dh = init_memory.shape[3]
    nblocks = count // BLOCK
    slice_rows = heads * dh // n_sp
    key_log = -0.5 * math.log(dh)
    me = lax.axis_index("sp")
    side = lax.axis_index("tp")
    other = 1 - side
    my_row = pl.multiple_of(side * own, own)
    peer_row = pl.multiple_of(other * own, own)
    my_head = (me * slice_rows) // dh
    my_depth = pl.multiple_of(me * slice_rows - my_head * dh, slice_rows)
    my_lane = pl.multiple_of(side * local_width, local_width)

    def local(src, dst, index):
        return pltpu.make_async_copy(src, dst, lsem.at[index])

    weights = (w_key, w_value, w_query, w_outgate, w_gatein, w_convin, w_gateout)

    barrier = pltpu.get_barrier_semaphore()
    pl.semaphore_signal(barrier, inc=1, device_id={"tp": other}, device_id_type=MESH)

    def greet(k, carry):
        pl.semaphore_signal(
            barrier, inc=1, device_id={"sp": lax.rem(me + k, n_sp)}, device_id_type=MESH
        )
        return carry

    lax.fori_loop(1, n_sp, greet, 0)

    first = [
        local(tokens.at[0], tok, L_TOK),
        local(norm_gain, gain, L_GAIN),
        local(w_igate, wig, L_WIG),
        local(w_fgate, wfg, L_WFG),
        local(w_key, w.at[K_], L_W + K_),
        local(w_value, w.at[V_], L_W + V_),
    ]
    later = [
        local(weights[p], w.at[p], L_W + p) for p in range(2, 7)
    ] + [
        local(forget_extra.at[0], fe, L_FE),
        local(input_bias, ib, L_IB),
        local(forget_bias, fb, L_FB),
        local(conv_taps, taps, L_TAPS),
        local(head_gain, hg, L_HG),
        local(init_memory.at[0, my_head, pl.ds(my_depth, slice_rows), :], init, L_INIT),
        local(out_memory, wo.at[pl.ds(0, local_width), :], L_OM),
        local(out_conv, wo.at[pl.ds(local_width, local_width), :], L_OC),
    ]
    for copy in first:
        copy.start()
    first[1].wait()
    first[0].wait()
    for copy in later:
        copy.start()

    gain_row = gain[...].astype(F32)
    step_rows = 64

    def norm_step(i, carry):
        rows = pl.multiple_of(i * step_rows, step_rows)
        values = tok[pl.ds(rows, step_rows), :].astype(F32)
        scale = lax.rsqrt(jnp.mean(values * values, axis=-1, keepdims=True) + EPSILON)
        x[pl.ds(my_row + rows, step_rows), :] = (values * scale * gain_row).astype(BF16)
        return carry

    lax.fori_loop(0, own // step_rows, norm_step, 0)

    first[2].wait()
    first[3].wait()
    narrow = wig.shape[1]
    wg[:, 0:narrow] = wig[...]
    wg[:, narrow : 2 * narrow] = wfg[...]
    wg[:, 2 * narrow :] = jnp.zeros((width, wg.shape[1] - 2 * narrow), BF16)

    def gate_dot(row):
        gates[pl.ds(row, own), :] = jnp.dot(
            x[pl.ds(row, own), :], wg[...], preferred_element_type=F32
        )

    def project(row, start, stop, wait):
        def step(p, carry):
            if wait:
                pltpu.make_async_copy(w_query, w.at[p], lsem.at[L_W + p]).wait()
            proj[p, pl.ds(row, own), :] = jnp.dot(
                x[pl.ds(row, own), :], w[p], preferred_element_type=F32
            ).astype(BF16)
            return carry

        lax.fori_loop(start, stop, step, 0)

    project(my_row, 0, 2, True)
    gate_dot(my_row)

    pl.semaphore_wait(barrier, n_sp)
    send_rows = pltpu.make_async_remote_copy(
        src_ref=x.at[pl.ds(my_row, own), :],
        dst_ref=x.at[pl.ds(my_row, own), :],
        send_sem=tok_s, recv_sem=tok_r,
        device_id={"tp": other}, device_id_type=MESH,
    )
    send_rows.start()
    project(my_row, 2, 7, True)
    take_rows = pltpu.make_async_remote_copy(
        src_ref=x.at[pl.ds(peer_row, own), :],
        dst_ref=x.at[pl.ds(peer_row, own), :],
        send_sem=tok_s, recv_sem=tok_r,
        device_id={"tp": other}, device_id_type=MESH,
    )
    take_rows.wait_recv()
    project(peer_row, 0, 2, False)
    gate_dot(peer_row)

    for copy in later[5:8]:
        copy.wait()
    lanes = lax.broadcasted_iota(jnp.int32, (nblocks * heads, BLOCK), 1)
    head_rows = lax.broadcasted_iota(jnp.int32, (heads, BLOCK), 0)
    bias_in = jnp.zeros((heads, BLOCK), F32)
    bias_forget = jnp.zeros((heads, BLOCK), F32)
    for h in range(heads):
        for part_index in range(2):
            pick = (head_rows == h) & (side == part_index)
            c = part_index * heads + h
            bias_in = jnp.where(pick, ib[0:1, c : c + 1], bias_in)
            bias_forget = jnp.where(pick, fb[0:1, c : c + 1], bias_forget)
    ins, forgets = [], []
    pad = jnp.zeros((BLOCK, BLOCK - heads), F32)
    for b in range(nblocks):
        turned = gates[b * BLOCK : (b + 1) * BLOCK, :].T
        extra = jnp.concatenate([fe[b * BLOCK : (b + 1) * BLOCK, :], pad], axis=1).T
        pre_in = jnp.where(side == 0, turned[0:heads], turned[heads : 2 * heads])
        pre_forget = jnp.where(
            side == 0, turned[2 * heads : 3 * heads], turned[3 * heads : 4 * heads]
        )
        ins.append(pre_in + bias_in)
        forget = pre_forget + bias_forget
        forgets.append(
            jnp.minimum(forget, 0.0) - jnp.log1p(jnp.exp(-jnp.abs(forget))) + extra[0:heads]
        )
    ins = jnp.concatenate(ins, axis=0)
    cumulative = jnp.concatenate(forgets, axis=0)
    shift = 1
    while shift < BLOCK:
        cumulative = cumulative + jnp.where(
            lanes >= shift, pltpu.roll(cumulative, shift, 1), 0.0
        )
        shift *= 2
    pair = ins - cumulative
    top = pair
    shift = 1
    while shift < BLOCK:
        top = jnp.maximum(top, jnp.where(lanes >= shift, pltpu.roll(top, shift, 1), top))
        shift *= 2
    total = jnp.broadcast_to(cumulative[:, BLOCK - 1 :], cumulative.shape)
    last_top = jnp.broadcast_to(top[:, BLOCK - 1 :], top.shape)
    log_scale = jnp.full((heads, BLOCK), LOWEST_LOG, F32)
    before = jnp.zeros((heads, BLOCK), F32)
    scales, befores, alphas, betas = [], [], [], []
    for b in range(nblocks):
        block_total = total[b * heads : (b + 1) * heads]
        block_top = block_total + last_top[b * heads : (b + 1) * heads]
        scales.append(log_scale)
        befores.append(before)
        merged = jnp.maximum(block_total + log_scale, block_top)
        alphas.append(jnp.exp(block_total + log_scale - merged))
        betas.append(jnp.exp(block_top - merged))
        log_scale = merged
        before = before + block_total
    scal[0:heads, :] = before
    scal[heads : 2 * heads, :] = log_scale
    scales = jnp.concatenate(scales, axis=0)
    row_top = jnp.maximum(scales, top)
    table[T_BIAS] = pair + key_log
    table[T_KW] = jnp.exp(pair + key_log - last_top)
    table[T_ALPHA] = jnp.concatenate(alphas, axis=0)
    table[T_BETA] = jnp.concatenate(betas, axis=0)
    table[T_TOP] = row_top
    table[T_CARRY] = jnp.concatenate(befores, axis=0)
    carry_weight = jnp.exp(scales - row_top)
    fill = jnp.zeros((BLOCK - 2 * heads, BLOCK), F32)
    for b in range(nblocks):
        rows = slice(b * heads, (b + 1) * heads)
        cols[b] = jnp.concatenate([row_top[rows], carry_weight[rows], fill], axis=0).T

    scal_in[me] = scal[...]

    def send_scales(k, carry):
        target = lax.rem(me + k, n_sp)
        pltpu.make_async_remote_copy(
            src_ref=scal, dst_ref=scal_in.at[me],
            send_sem=scal_s.at[target], recv_sem=scal_r.at[me],
            device_id={"sp": target}, device_id_type=MESH,
        ).start()
        return carry

    lax.fori_loop(1, n_sp, send_scales, 0)

    for h in range(heads):
        mix[h] = jnp.zeros((dh, dh), F32)

    def terms_step(b, carry):
        rows = pl.ds(pl.multiple_of(b * BLOCK, BLOCK), BLOCK)
        for h in range(heads):
            at = pl.ds(b * heads + h, 1)
            hs = slice(h * dh, (h + 1) * dh)
            turned = proj[K_, rows, hs].T
            keys_t[b, h] = turned
            weighted = (turned.astype(F32) * table[T_KW, at, :]).astype(BF16)
            terms = jnp.dot(weighted, proj[V_, rows, hs], preferred_element_type=F32)
            held = mix[h]
            prefix[b, h] = held.astype(BF16)
            mix[h] = table[T_ALPHA, at, :] * held + table[T_BETA, at, :] * terms
        return carry

    lax.fori_loop(0, nblocks, terms_step, 0)
    for h in range(heads):
        per_head = dh // slice_rows
        for piece in range(per_head):
            seg[h * per_head + piece] = mix[
                h, piece * slice_rows : (piece + 1) * slice_rows, :
            ].astype(BF16)
    seg_in[me] = seg[me]

    def send_segment(k, carry):
        target = lax.rem(me + k, n_sp)
        pltpu.make_async_remote_copy(
            src_ref=seg.at[target], dst_ref=seg_in.at[me],
            send_sem=seg_s.at[target], recv_sem=seg_r.at[me],
            device_id={"sp": target}, device_id_type=MESH,
        ).start()
        return carry

    lax.fori_loop(1, n_sp, send_segment, 0)

    project(peer_row, GI_, GO_, False)
    conv_rows = 64

    def product_step(i, carry):
        rows = pl.multiple_of(i * conv_rows, conv_rows)
        conv[pl.ds(rows + 8, conv_rows), :] = (
            (
                proj[GI_, pl.ds(rows, conv_rows), :].astype(F32)
                * proj[CI_, pl.ds(rows, conv_rows), :].astype(F32)
            )
            .astype(BF16)
            .astype(F32)
        )
        return carry

    lax.fori_loop(0, count // conv_rows, product_step, 0)
    following = lax.rem(me + 1, n_sp)
    rim = pltpu.make_async_remote_copy(
        src_ref=conv.at[pl.ds(count, 8), :], dst_ref=rim_in,
        send_sem=rim_s, recv_sem=rim_r,
        device_id={"sp": following}, device_id_type=MESH,
    )
    rim.start()
    project(peer_row, Q_, GI_, False)

    def wait_from(src, dst, send, recv):
        def step(k, carry):
            source = lax.rem(me + k, n_sp)
            pltpu.make_async_remote_copy(
                src_ref=src.at[source] if src is not scal else src,
                dst_ref=dst.at[source],
                send_sem=send.at[source], recv_sem=recv.at[source],
                device_id={"sp": source}, device_id_type=MESH,
            ).wait_recv()
            return carry

        lax.fori_loop(1, n_sp, step, 0)

    wait_from(scal, scal_in, scal_s, scal_r)
    wait_from(seg, seg_in, seg_s, seg_r)
    later[10].wait()
    state = init[...]
    state_log = jnp.zeros((1, BLOCK), F32)
    for i in range(n_sp):
        state_out[i] = state.astype(BF16)
        if i == n_sp - 1:
            break
        span = scal_in[i, pl.ds(my_head, 1), :]
        span_top = scal_in[i, pl.ds(heads + my_head, 1), :]
        merged = jnp.maximum(span + state_log, span_top)
        state = (
            jnp.exp(span + state_log - merged) * state
            + jnp.exp(span_top - merged) * seg_in[i].astype(F32)
        )
        state_log = merged
    state_in[me] = state_out[me]

    def send_state(k, carry):
        target = lax.rem(me + k, n_sp)
        pltpu.make_async_remote_copy(
            src_ref=state_out.at[target], dst_ref=state_in.at[me],
            send_sem=st_s.at[target], recv_sem=st_r.at[me],
            device_id={"sp": target}, device_id_type=MESH,
        ).start()
        return carry

    lax.fori_loop(1, n_sp, send_state, 0)
    project(peer_row, GO_, GO_ + 1, False)

    start_log = jnp.zeros((heads, BLOCK), F32)
    for i in range(n_sp - 1):
        merged = jnp.maximum(scal_in[i, 0:heads, :] + start_log, scal_in[i, heads : 2 * heads, :])
        start_log = jnp.where(i < me, merged, start_log)

    t_index = lax.broadcasted_iota(jnp.int32, (BLOCK, BLOCK), 0)
    s_index = lax.broadcasted_iota(jnp.int32, (BLOCK, BLOCK), 1)
    causal = s_index <= t_index
    later[9].wait()
    later[8].wait()
    head_row = hg[:, pl.ds(my_lane, local_width)].astype(F32)

    def read_step(b, carry):
        rows = pl.ds(pl.multiple_of(b * BLOCK, BLOCK), BLOCK)
        columns = cols[b]
        for h in range(heads):
            at = pl.ds(b * heads + h, 1)
            hs = slice(h * dh, (h + 1) * dh)
            query = proj[Q_, rows, hs]
            scores = jnp.dot(query, keys_t[b, h], preferred_element_type=F32)
            log_weight = jnp.where(
                causal, table[T_BIAS, at, :] - columns[:, h : h + 1], -jnp.inf
            )
            weighted = (jnp.exp(log_weight) * scores).astype(BF16)
            read[rows, hs] = jnp.dot(
                weighted, proj[V_, rows, hs], preferred_element_type=F32
            ) + columns[:, heads + h : heads + h + 1] * jnp.dot(
                query, prefix[b, h], preferred_element_type=F32
            )
        sig[rows, :] = head_row * jax.nn.sigmoid(proj[OG_, rows, :].astype(F32))
        return carry

    lax.fori_loop(0, nblocks, read_step, 0)

    pltpu.make_async_remote_copy(
        src_ref=conv.at[pl.ds(count, 8), :], dst_ref=rim_in,
        send_sem=rim_s, recv_sem=rim_r,
        device_id={"sp": following}, device_id_type=MESH,
    ).wait_recv()
    conv[0:8, :] = jnp.where(me == 0, 0.0, rim_in[...])
    tap_rows = taps[:, pl.ds(my_lane, local_width)].astype(F32)

    def conv_step(i, carry):
        rows = pl.multiple_of(i * conv_rows, conv_rows)
        window = conv[pl.ds(rows, conv_rows + 8), :]
        mixed = window[6 : 6 + conv_rows] * tap_rows[0:1]
        mixed = mixed + window[7 : 7 + conv_rows] * tap_rows[1:2]
        mixed = mixed + window[8 : 8 + conv_rows] * tap_rows[2:3]
        both[pl.ds(rows, conv_rows), local_width:] = (
            proj[GO_, pl.ds(rows, conv_rows), :].astype(F32) * mixed
        ).astype(BF16)
        return carry

    lax.fori_loop(0, count // conv_rows, conv_step, 0)

    carried_log = table[T_CARRY] + jnp.concatenate([start_log] * nblocks, axis=0)
    new_top = jnp.maximum(table[T_TOP], carried_log)
    keep = jnp.exp(table[T_TOP] - new_top)
    bring = jnp.exp(carried_log - new_top)
    for b in range(nblocks):
        rows = slice(b * heads, (b + 1) * heads)
        cols[b] = jnp.concatenate([keep[rows], bring[rows], fill], axis=0).T
    wait_from(state_out, state_in, st_s, st_r)
    later[11].wait()
    later[12].wait()
    per_head = dh // slice_rows

    def finish_rows(row):
        def step(i, carry):
            b = row // BLOCK + i
            rows = pl.ds(pl.multiple_of(b * BLOCK, BLOCK), BLOCK)
            columns = cols[b]
            for h in range(heads):
                hs = slice(h * dh, (h + 1) * dh)
                start = state_in[h * per_head : (h + 1) * per_head].reshape(dh, dh)
                readout = columns[:, h : h + 1] * read[rows, hs] + columns[
                    :, heads + h : heads + h + 1
                ] * jnp.dot(proj[Q_, rows, hs], start, preferred_element_type=F32)
                normalized = readout * lax.rsqrt(
                    jnp.mean(readout * readout, axis=-1, keepdims=True) + EPSILON
                )
                both[rows, hs] = (normalized * sig[rows, hs]).astype(BF16)
            return carry

        lax.fori_loop(0, own // BLOCK, step, 0)

    finish_rows(peer_row)
    pieces = 2
    piece_rows = own // pieces

    def send_part(i):
        return pltpu.make_async_remote_copy(
            src_ref=part.at[pl.ds(i * piece_rows, piece_rows), :],
            dst_ref=part_in.at[pl.ds(i * piece_rows, piece_rows), :],
            send_sem=out_s.at[i], recv_sem=out_r.at[i],
            device_id={"tp": other}, device_id_type=MESH,
        )

    for i in range(pieces):
        part[pl.ds(i * piece_rows, piece_rows), :] = jnp.dot(
            both[pl.ds(peer_row + i * piece_rows, piece_rows), :], wo[...],
            preferred_element_type=F32,
        ).astype(BF16)
        send_part(i).start()
    finish_rows(my_row)
    stores = []
    for i in range(pieces):
        mine = jnp.dot(
            both[pl.ds(my_row + i * piece_rows, piece_rows), :], wo[...],
            preferred_element_type=F32,
        ).astype(BF16)
        rows = pl.ds(i * piece_rows, piece_rows)
        send_part(i).wait_recv()
        tok[rows, :] = (mine.astype(F32) + part_in[rows, :].astype(F32)).astype(BF16)
        store = local(tok.at[rows, :], out.at[0, rows, :], L_OUT + i)
        store.start()
        stores.append(store)

    send_rows.wait_send()
    rim.wait_send()

    def drain(k, carry):
        target = lax.rem(me + k, n_sp)
        for src, send, recv, dst in (
            (scal, scal_s, scal_r, scal_in.at[me]),
            (seg.at[target], seg_s, seg_r, seg_in.at[me]),
            (state_out.at[target], st_s, st_r, state_in.at[me]),
        ):
            pltpu.make_async_remote_copy(
                src_ref=src, dst_ref=dst,
                send_sem=send.at[target], recv_sem=recv.at[me],
                device_id={"sp": target}, device_id_type=MESH,
            ).wait_send()
        return carry

    lax.fori_loop(1, n_sp, drain, 0)
    for i in range(pieces):
        send_part(i).wait_send()
    for store in stores:
        store.wait()


def local_layer(
    n_sp,
    tokens, norm_gain, w_query, w_key, w_value, w_outgate, w_gatein, w_gateout, w_convin,
    w_igate, w_fgate, input_bias, forget_bias, forget_extra, init_memory, head_gain, conv_taps,
    out_memory, out_conv,
):
    own, width = tokens.shape[1:]
    count = 2 * own
    local_width = w_query.shape[1]
    heads, dh = init_memory.shape[1], init_memory.shape[3]
    nblocks = count // BLOCK
    slice_rows = heads * dh // n_sp
    vmem = pltpu.VMEM
    dma = pltpu.SemaphoreType.DMA
    scratch = [
        vmem((own, width), BF16),
        vmem((1, width), BF16),
        vmem((count, width), BF16),
        vmem((7, width, local_width), BF16),
        vmem((2 * local_width, width), BF16),
        vmem(w_igate.shape, BF16),
        vmem(w_fgate.shape, BF16),
        vmem((width, 128), BF16),
        vmem((7, count, local_width), BF16),
        vmem((count, 128), F32),
        vmem((count, heads), F32),
        vmem((1, 2 * heads), F32),
        vmem((1, 2 * heads), F32),
        vmem(conv_taps.shape, BF16),
        vmem((1, 2 * local_width), BF16),
        vmem((slice_rows, dh), F32),
        vmem((nblocks, heads, dh, BLOCK), BF16),
        vmem((nblocks, heads, dh, dh), BF16),
        vmem((6, nblocks * heads, BLOCK), F32),
        vmem((nblocks, BLOCK, BLOCK), F32),
        vmem((heads, dh, dh), F32),
        vmem((n_sp, slice_rows, dh), BF16),
        vmem((n_sp, slice_rows, dh), BF16),
        vmem((2 * heads, BLOCK), F32),
        vmem((n_sp, 2 * heads, BLOCK), F32),
        vmem((n_sp, slice_rows, dh), BF16),
        vmem((n_sp, slice_rows, dh), BF16),
        vmem((8, local_width), F32),
        vmem((count, local_width), F32),
        vmem((count, local_width), F32),
        vmem((count + 8, local_width), F32),
        vmem((count, 2 * local_width), BF16),
        vmem((own, width), BF16),
        vmem((own, width), BF16),
        dma((L_W + 7,)),
        dma, dma,
        dma((n_sp,)), dma((n_sp,)),
        dma((n_sp,)), dma((n_sp,)),
        dma((n_sp,)), dma((n_sp,)),
        dma, dma,
        dma((2,)), dma((2,)),
    ]
    return pl.pallas_call(
        functools.partial(kernel, n_sp),
        out_shape=jax.ShapeDtypeStruct(tokens.shape, BF16),
        in_specs=[pl.BlockSpec(memory_space=pl.ANY)] * 19,
        out_specs=pl.BlockSpec(memory_space=pl.ANY),
        scratch_shapes=scratch,
        compiler_params=pltpu.CompilerParams(
            collective_id=0, has_side_effects=True, vmem_limit_bytes=67043328
        ),
    )(
        tokens, norm_gain.reshape(1, -1),
        w_query, w_key, w_value, w_outgate, w_gatein, w_gateout, w_convin,
        w_igate, w_fgate, input_bias.reshape(1, -1), forget_bias.reshape(1, -1),
        forget_extra, init_memory, head_gain.reshape(1, -1), conv_taps, out_memory, out_conv,
    )


def solution(mesh):
    rows = P("fs", ("sp", "tp"), None)
    column, replicated = P(None, "tp"), P()
    return jax.shard_map(
        functools.partial(local_layer, mesh.shape["sp"]),
        mesh=mesh,
        in_specs=(
            rows, replicated,
            column, column, column, column, column, column, column,
            replicated, replicated, replicated, replicated,
            P("fs", "sp", "tp"), P("fs", "tp", None, None),
            replicated, replicated,
            P("tp", None), P("tp", None),
        ),
        out_specs=rows,
        check_vma=False,
    )
```

time: 204 us -> 58.1 us (0.28)
  matrix products: 63.3 us -> 0 us
  Pallas kernels: 0 us -> 46.5 us
  other arithmetic: 37.2 us -> 0 us
  blocking collectives: 36.3 us -> 0 us
  waiting for transfers between devices: 34.3 us -> 0 us
  between operations: 14.4 us -> 0.01 us
  starting transfers between devices: 3.28 us -> 0 us
  local copies, waits for them, and re-layouts: 14 us -> 11 us
    dot_general x11 -> x0, matrix products: 63.3 us -> none  [the longest x5 23.3 us: project(): jnp.dot(normed_all, weight, preferred_element_type=jnp.float32)]
    pallas_call x0 -> x1, Pallas kernels: none -> 46.5 us  [local_layer(): pl.pallas_call(functools.partial(kernel, n_sp), out_shape=jax.ShapeDtypeS...]
    all_gather x3 -> x0, waiting for transfers between devices: 34.2 us -> none  [the longest x1 18 us: local(): normed_all = lax.all_gather(normed, 'tp', axis=0, tiled=True)]
    all_to_all x1 -> x0, blocking collectives: 14.2 us -> none  [sum_at_owner(): blocks = lax.all_to_all(in_blocks(value, dim, size), axis, 0, 0, tiled=True)]
    all_gather x2 -> x0, blocking collectives: 13.3 us -> none  [prefix_by_axis(): pieces = jax.tree.map(lambda part: lax.all_gather(part, axis), subtotal)]
    add x10 -> x0, other arithmetic: 10.5 us -> none  [the longest x9 10.5 us: compose(): kept_share[..., None, None] * memory]
    unnamed x1 -> x0, blocking collectives: 8.84 us -> none
    reshape x6 -> x2, local copies, waits for them, and re-layouts: 10.4 us -> 2.55 us  [the longest x1 1.29 us: local_layer(): norm_gain.reshape(1, -1)]
  transfers between devices with their start and end apart: 4 -> 0, of which waited for: 2 -> 0; matrix products, arithmetic and copies ran while one was open for 27% -> 0% of each run, Pallas kernels for 0% -> 0%
where the time goes in v1:
time: 58.1 us; the launch traced here: 57.5 us
  Pallas kernels  46.5 us (80%)
  local copies, waits for them, and re-layouts  11 us (19%)
    pallas_call x1, Pallas kernels, local_layer(): pl.pallas_call(functools.partial(kernel, n_sp), out_shape=jax.ShapeDtypeS...  46.5 us
    unnamed x4, local copies, waits for them, and re-layouts  8.44 us
    reshape x1, local copies, waits for them, and re-layouts, local_layer(): norm_gain.reshape(1, -1)  1.29 us
    reshape x1, local copies, waits for them, and re-layouts, local_layer(): head_gain.reshape(1, -1)  1.27 us

profile of v1, /device:TPU:1, one launch (start us, length us, event | category | flops | bytes accessed | tf_op | source)
XLA Modules:
  0.0 57.5 jit_solution(1339425920690079271)
XLA Ops:
  0.0 1.3 %reshape.15.head_gain = bf16[1,1024]{1,0:T(2,128)(2,1)} reshape(bf16[1024]{0:T(1024)(128)(2,1)} %param.34) | data formatting | bytes 4096 | tf_op jit(solution)/shard_map/reshape | solution.py:556
  1.3 1.3 %reshape.12.norm_gain = bf16[1,2048]{1,0:T(2,128)(2,1)} reshape(bf16[2048]{0:T(1024)(128)(2,1)} %param.20) | data formatting | bytes 8192 | tf_op jit(solution)/shard_map/reshape | solution.py:553
  2.6 1.8 %copy.20.w_igate = bf16[2048,8]{1,0:T(8,128)(2,1)} copy(bf16[2048,8]{0,1:T(8,128)(2,1)} %param.28) | data formatting | bytes 65536 | tf_op args[9]
  4.3 1.8 %copy.21.w_fgate = bf16[2048,8]{1,0:T(8,128)(2,1)} copy(bf16[2048,8]{0,1:T(8,128)(2,1)} %param.29) | data formatting | bytes 65536 | tf_op args[10]
  6.1 1.8 %copy.22.forget_extra = f32[1,1024,4]{2,1,0:T(8,128)} copy(f32[1,1024,4]{1,2,0:T(4,128)} %param.32) | data formatting | bytes 32768 | tf_op args[13]
  7.8 46.5 %shard_map.181 = bf16[1,512,2048]{2,1,0:T(8,128)(2,1)} custom-call(bf16[1,512,2048]{2,1,0:T(8,128)(2,1)} %tokens.1, bf16[1,2048]{1,0:T(2,128)(2,1)} %reshape.12.norm_gain, bf16[2048,512]{1,0:T(8,128)(2,1)} %w_query.1, bf16[2048,512]{1,0:T(8,128)(2,1)} %w_key.1, bf16[2048,512]{1,0:T(8,128)(2,1)} %w_value.1, bf16[2048,512]{1,0:T(8,128)(2,1)} %w_outgate.1, ...), custom_call_target="tpu_custom_call" | custom-call | tf_op jit(solution)/shard_map/pallas_call | solution.py:543
  54.4 3.2 %copy.24 = bf16[1,512,2048]{2,1,0:T(8,128)(2,1)} copy(bf16[1,512,2048]{2,1,0:T(8,128)(2,1)} %shard_map.181) | data formatting | bytes 4194304

commit v2 on v1

v2 whole, which is shorter than its diff:
```python
import functools
import math

import jax
import jax.numpy as jnp
from jax import lax
from jax.experimental import pallas as pl
from jax.experimental.pallas import tpu as pltpu
from jax.sharding import PartitionSpec as P

MESH = pl.DeviceIdType.MESH
F32 = jnp.float32
BF16 = jnp.bfloat16
BLOCK = 128
EPSILON = 1e-06
LOWEST_LOG = -1e30

K_, V_, Q_, OG_, GI_, CI_, GO_ = range(7)
T_BIAS, T_KW, T_ALPHA, T_BETA, T_TOP, T_CARRY = range(6)
L_TOK, L_WIG, L_WFG, L_GAIN, L_FE, L_IB, L_FB, L_TAPS, L_HG, L_OM, L_OC, L_INIT, L_W = (
    0, 4, 5, 6, 7, 8, 9, 10, 11, 12, 13, 14, 16,
)


def kernel(
    n_sp,
    tokens, norm_gain, w_query, w_key, w_value, w_outgate, w_gatein, w_gateout, w_convin,
    w_igate, w_fgate, input_bias, forget_bias, forget_extra, init_memory, head_gain, conv_taps,
    out_memory, out_conv,
    out,
    tok, gain, x, w, wo, wig, wfg, proj, gates, fe, ib, fb, taps, hg, init,
    keys_t, prefix, table, cols, terms, seg, seg_in, scal, scal_in, state_out, state_in,
    rim_in, read, sig, prod, both, acc, part, part_in,
    lsem, tok_s, tok_r, gate_s, gate_r, seg_s, seg_r, scal_s, scal_r, st_s, st_r, rim_s, rim_r,
    out_s, out_r,
):
    own = tokens.shape[1]
    width = tokens.shape[2]
    count = 2 * own
    local_width = w_query.shape[1]
    heads = init_memory.shape[1]
    dh = init_memory.shape[3]
    nblocks = count // BLOCK
    half_blocks = nblocks // 2
    slice_rows = heads * dh // n_sp
    per_head = dh // slice_rows
    key_log = -0.5 * math.log(dh)
    me = lax.axis_index("sp")
    side = lax.axis_index("tp")
    other = 1 - side
    my_row = pl.multiple_of(side * own, own)
    peer_row = pl.multiple_of(other * own, own)
    my_block = side * half_blocks
    peer_block = other * half_blocks
    my_head = (me * slice_rows) // dh
    my_depth = pl.multiple_of(me * slice_rows - my_head * dh, slice_rows)
    my_lane = pl.multiple_of(side * local_width, local_width)
    my_rows = pl.ds(my_row, own)
    peer_rows = pl.ds(peer_row, own)

    def local(src, dst, index):
        return pltpu.make_async_copy(src, dst, lsem.at[index])

    weights = (w_key, w_value, w_query, w_outgate, w_gatein, w_convin, w_gateout)

    barrier = pltpu.get_barrier_semaphore()
    chunks = 4
    chunk_rows = own // chunks
    token_copies = [
        local(
            tokens.at[0, pl.ds(c * chunk_rows, chunk_rows), :],
            tok.at[pl.ds(c * chunk_rows, chunk_rows), :],
            L_TOK + c,
        )
        for c in range(chunks)
    ]
    gain_copy = local(norm_gain, gain, L_GAIN)
    narrow_copies = [local(w_igate, wig, L_WIG), local(w_fgate, wfg, L_WFG)]
    w_copies = [local(weights[p], w.at[p], L_W + p) for p in range(7)]
    gate_copies = [
        local(forget_extra.at[0], fe, L_FE),
        local(input_bias, ib, L_IB),
        local(forget_bias, fb, L_FB),
    ]
    head_copy = local(head_gain, hg, L_HG)
    taps_copy = local(conv_taps, taps, L_TAPS)
    init_copy = local(init_memory.at[0, my_head, pl.ds(my_depth, slice_rows), :], init, L_INIT)
    out_copies = [
        local(out_conv, wo.at[pl.ds(local_width, local_width), :], L_OC),
        local(out_memory, wo.at[pl.ds(0, local_width), :], L_OM),
    ]
    gain_copy.start()
    for copy in token_copies + narrow_copies + w_copies[:2]:
        copy.start()
    pl.semaphore_signal(barrier, inc=1, device_id={"tp": other}, device_id_type=MESH)

    def greet(k, carry):
        pl.semaphore_signal(
            barrier, inc=1, device_id={"sp": lax.rem(me + k, n_sp)}, device_id_type=MESH
        )
        return carry

    lax.fori_loop(1, n_sp, greet, 0)

    gain_copy.wait()
    gain_row = jnp.concatenate(
        [gain[i : i + 1, :] for i in range(gain.shape[0])], axis=1
    ).astype(F32)
    step_rows = 64
    for c in range(chunks):
        token_copies[c].wait()
        if c == chunks - 1:
            for copy in w_copies[2:] + gate_copies + [head_copy, taps_copy, init_copy]:
                copy.start()
            for copy in out_copies:
                copy.start()

        def norm_step(i, carry):
            rows = pl.multiple_of(c * chunk_rows + i * step_rows, step_rows)
            values = tok[pl.ds(rows, step_rows), :].astype(F32)
            scale = lax.rsqrt(jnp.mean(values * values, axis=-1, keepdims=True) + EPSILON)
            x[pl.ds(my_row + rows, step_rows), :] = (values * scale * gain_row).astype(BF16)
            return carry

        lax.fori_loop(0, chunk_rows // step_rows, norm_step, 0)

    def project(p, row):
        return jnp.dot(
            x[pl.ds(row, own), :], w[p], preferred_element_type=F32
        ).astype(BF16)

    def project_sig(row):
        value = project(OG_, row).astype(F32)
        gains = hg[...].astype(F32)
        gains = jnp.where(side == 0, gains[0:heads], gains[heads : 2 * heads])
        head_row = jnp.concatenate([gains[i : i + 1] for i in range(heads)], axis=1)
        sig[pl.ds(row, own), :] = head_row * jax.nn.sigmoid(value)

    def project_prod(row):
        value = project(CI_, row).astype(F32)
        prod[pl.ds(row + 16, own), :] = (
            proj[GI_, pl.ds(row, own), :].astype(F32) * value
        ).astype(BF16)

    for copy in narrow_copies:
        copy.wait()
    narrow = jnp.concatenate([wig[...], wfg[...]], axis=0)
    w_copies[K_].wait()
    gates[:, my_rows] = lax.dot_general(
        narrow, x[my_rows, :], (((1,), (1,)), ((), ())), preferred_element_type=F32
    )
    proj[K_, my_rows, :] = project(K_, my_row)

    pl.semaphore_wait(barrier, n_sp)
    peer = dict(device_id={"tp": other}, device_id_type=MESH)
    send_rows = pltpu.make_async_remote_copy(
        src_ref=x.at[my_rows, :], dst_ref=x.at[my_rows, :],
        send_sem=tok_s, recv_sem=tok_r, **peer,
    )
    take_rows = pltpu.make_async_remote_copy(
        src_ref=x.at[peer_rows, :], dst_ref=x.at[peer_rows, :],
        send_sem=tok_s, recv_sem=tok_r, **peer,
    )
    send_gates = pltpu.make_async_remote_copy(
        src_ref=gates.at[:, my_rows], dst_ref=gates.at[:, my_rows],
        send_sem=gate_s, recv_sem=gate_r, **peer,
    )
    take_gates = pltpu.make_async_remote_copy(
        src_ref=gates.at[:, peer_rows], dst_ref=gates.at[:, peer_rows],
        send_sem=gate_s, recv_sem=gate_r, **peer,
    )
    send_gates.start()
    send_rows.start()

    w_copies[V_].wait()
    w_copies[Q_].wait()
    proj[V_, my_rows, :] = project(V_, my_row)
    proj[Q_, my_rows, :] = project(Q_, my_row)
    w_copies[OG_].wait()
    w_copies[GI_].wait()
    head_copy.wait()
    for copy in gate_copies:
        copy.wait()
    take_gates.wait_recv()

    lanes = lax.broadcasted_iota(jnp.int32, (nblocks * heads, BLOCK), 1)
    head_rows = lax.broadcasted_iota(jnp.int32, (heads, BLOCK), 0)
    bias_in = jnp.zeros((heads, BLOCK), F32)
    bias_forget = jnp.zeros((heads, BLOCK), F32)
    for h in range(heads):
        for part_index in range(2):
            pick = (head_rows == h) & (side == part_index)
            c = part_index * heads + h
            bias_in = jnp.where(pick, ib[0:1, c : c + 1], bias_in)
            bias_forget = jnp.where(pick, fb[0:1, c : c + 1], bias_forget)
    ins, forgets = [], []
    for b in range(nblocks):
        at = slice(b * BLOCK, (b + 1) * BLOCK)
        pre = gates[:, at]
        ins.append(jnp.where(side == 0, pre[0:heads], pre[heads : 2 * heads]) + bias_in)
        forget = (
            jnp.where(side == 0, pre[2 * heads : 3 * heads], pre[3 * heads : 4 * heads])
            + bias_forget
        )
        forgets.append(
            jnp.minimum(forget, 0.0) - jnp.log1p(jnp.exp(-jnp.abs(forget))) + fe[:, at]
        )
    ins = jnp.concatenate(ins, axis=0)
    cumulative = jnp.concatenate(forgets, axis=0)
    shift = 1
    while shift < BLOCK:
        cumulative = cumulative + jnp.where(
            lanes >= shift, pltpu.roll(cumulative, shift, 1), 0.0
        )
        shift *= 2
    pair = ins - cumulative
    top = pair
    shift = 1
    while shift < BLOCK:
        top = jnp.maximum(top, jnp.where(lanes >= shift, pltpu.roll(top, shift, 1), top))
        shift *= 2
    total = jnp.broadcast_to(cumulative[:, BLOCK - 1 :], cumulative.shape)
    last_top = jnp.broadcast_to(top[:, BLOCK - 1 :], top.shape)
    log_scale = jnp.full((heads, BLOCK), LOWEST_LOG, F32)
    before = jnp.zeros((heads, BLOCK), F32)
    scales, befores, alphas, betas = [], [], [], []
    for b in range(nblocks):
        block_total = total[b * heads : (b + 1) * heads]
        block_top = block_total + last_top[b * heads : (b + 1) * heads]
        scales.append(log_scale)
        befores.append(before)
        merged = jnp.maximum(block_total + log_scale, block_top)
        alphas.append(block_total + log_scale - merged)
        betas.append(block_top - merged)
        log_scale = merged
        before = before + block_total
    scal[0:heads, :] = before
    scal[heads : 2 * heads, :] = log_scale
    scal_in[me] = scal[...]
    scales = jnp.concatenate(scales, axis=0)
    row_top = jnp.maximum(scales, top)
    table[T_BIAS] = pair + key_log
    table[T_KW] = jnp.exp(pair + key_log - last_top)
    table[T_ALPHA] = jnp.exp(jnp.concatenate(alphas, axis=0))
    table[T_BETA] = jnp.exp(jnp.concatenate(betas, axis=0))
    table[T_TOP] = row_top
    table[T_CARRY] = jnp.concatenate(befores, axis=0)
    carry_weight = jnp.exp(scales - row_top)
    fill = jnp.zeros((BLOCK - 2 * heads, BLOCK), F32)
    for b in range(nblocks):
        rows = slice(b * heads, (b + 1) * heads)
        cols[b] = jnp.concatenate([row_top[rows], carry_weight[rows], fill], axis=0).T
    project_sig(my_row)
    proj[GI_, my_rows, :] = project(GI_, my_row)

    def send_scales(k, carry):
        target = lax.rem(me + k, n_sp)
        pltpu.make_async_remote_copy(
            src_ref=scal, dst_ref=scal_in.at[me],
            send_sem=scal_s.at[target], recv_sem=scal_r.at[me],
            device_id={"sp": target}, device_id_type=MESH,
        ).start()
        return carry

    lax.fori_loop(1, n_sp, send_scales, 0)

    def block_terms(first):
        for i in range(half_blocks):
            b = first + i
            rows = pl.ds(pl.multiple_of(b * BLOCK, BLOCK), BLOCK)
            for h in range(heads):
                hs = slice(h * dh, (h + 1) * dh)
                turned = proj[K_, rows, hs].T
                keys_t[b, h] = turned
                weighted = (
                    turned.astype(F32) * table[T_KW, pl.ds(b * heads + h, 1), :]
                ).astype(BF16)
                terms[b, h] = jnp.dot(weighted, proj[V_, rows, hs], preferred_element_type=F32)

    take_rows.wait_recv()
    block_terms(my_block)
    proj[K_, peer_rows, :] = project(K_, peer_row)
    proj[V_, peer_rows, :] = project(V_, peer_row)

    w_copies[CI_].wait()
    w_copies[GO_].wait()
    block_terms(peer_block)
    for h in range(heads):
        held = jnp.zeros((dh, dh), F32)
        for b in range(nblocks):
            at = pl.ds(b * heads + h, 1)
            prefix[b, h] = held.astype(BF16)
            held = table[T_ALPHA, at, :] * held + table[T_BETA, at, :] * terms[b, h]
        for piece in range(per_head):
            seg[h * per_head + piece] = held[
                piece * slice_rows : (piece + 1) * slice_rows, :
            ].astype(BF16)
    project_prod(my_row)

    seg_in[me] = seg[me]

    def send_segment(k, carry):
        target = lax.rem(me + k, n_sp)
        pltpu.make_async_remote_copy(
            src_ref=seg.at[target], dst_ref=seg_in.at[me],
            send_sem=seg_s.at[target], recv_sem=seg_r.at[me],
            device_id={"sp": target}, device_id_type=MESH,
        ).start()
        return carry

    lax.fori_loop(1, n_sp, send_segment, 0)

    proj[GI_, peer_rows, :] = project(GI_, peer_row)
    project_prod(peer_row)
    following = lax.rem(me + 1, n_sp)
    rim = pltpu.make_async_remote_copy(
        src_ref=prod.at[pl.ds(count, 16), :], dst_ref=rim_in,
        send_sem=rim_s, recv_sem=rim_r,
        device_id={"sp": following}, device_id_type=MESH,
    )
    rim.start()

    t_index = lax.broadcasted_iota(jnp.int32, (BLOCK, BLOCK), 0)
    s_index = lax.broadcasted_iota(jnp.int32, (BLOCK, BLOCK), 1)
    causal = s_index <= t_index

    def read_blocks(first):
        for i in range(half_blocks):
            b = first + i
            rows = pl.ds(pl.multiple_of(b * BLOCK, BLOCK), BLOCK)
            columns = cols[b]
            for h in range(heads):
                at = pl.ds(b * heads + h, 1)
                hs = slice(h * dh, (h + 1) * dh)
                query = proj[Q_, rows, hs]
                scores = jnp.dot(query, keys_t[b, h], preferred_element_type=F32)
                log_weight = jnp.where(
                    causal, table[T_BIAS, at, :] - columns[:, h : h + 1], -jnp.inf
                )
                weighted = (jnp.exp(log_weight) * scores).astype(BF16)
                read[rows, hs] = jnp.dot(
                    weighted, proj[V_, rows, hs], preferred_element_type=F32
                ) + columns[:, heads + h : heads + h + 1] * jnp.dot(
                    query, prefix[b, h], preferred_element_type=F32
                )

    read_blocks(my_block)
    proj[Q_, peer_rows, :] = project(Q_, peer_row)
    project_sig(peer_row)

    read_blocks(peer_block)
    proj[GO_, my_rows, :] = project(GO_, my_row)
    proj[GO_, peer_rows, :] = project(GO_, peer_row)

    def wait_from(src, dst, send, recv):
        def step(k, carry):
            source = lax.rem(me + k, n_sp)
            pltpu.make_async_remote_copy(
                src_ref=src.at[source] if src is not scal else src,
                dst_ref=dst.at[source],
                send_sem=send.at[source], recv_sem=recv.at[source],
                device_id={"sp": source}, device_id_type=MESH,
            ).wait_recv()
            return carry

        lax.fori_loop(1, n_sp, step, 0)

    init_copy.wait()
    wait_from(scal, scal_in, scal_s, scal_r)
    wait_from(seg, seg_in, seg_s, seg_r)

    state = init[...]
    state_log = jnp.zeros((1, BLOCK), F32)
    for i in range(n_sp):
        state_out[i] = state.astype(BF16)
        if i == n_sp - 1:
            break
        span = scal_in[i, pl.ds(my_head, 1), :]
        span_top = scal_in[i, pl.ds(heads + my_head, 1), :]
        merged = jnp.maximum(span + state_log, span_top)
        state = (
            jnp.exp(span + state_log - merged) * state
            + jnp.exp(span_top - merged) * seg_in[i].astype(F32)
        )
        state_log = merged
    state_in[me] = state_out[me]

    def send_state(k, carry):
        target = lax.rem(me + k, n_sp)
        pltpu.make_async_remote_copy(
            src_ref=state_out.at[target], dst_ref=state_in.at[me],
            send_sem=st_s.at[target], recv_sem=st_r.at[me],
            device_id={"sp": target}, device_id_type=MESH,
        ).start()
        return carry

    lax.fori_loop(1, n_sp, send_state, 0)

    taps_copy.wait()
    pltpu.make_async_remote_copy(
        src_ref=prod.at[pl.ds(count, 16), :], dst_ref=rim_in,
        send_sem=rim_s, recv_sem=rim_r,
        device_id={"sp": following}, device_id_type=MESH,
    ).wait_recv()
    for copy in out_copies:
        copy.wait()
    prod[0:16, :] = jnp.where(me == 0, jnp.zeros_like(rim_in), rim_in[...])
    tap_rows = taps[:, pl.ds(my_lane, local_width)].astype(F32)
    conv_rows = 64

    def convolve(first):
        for i in range(own // conv_rows):
            row = pl.multiple_of(first + i * conv_rows, conv_rows)
            window = prod[pl.ds(row, conv_rows + 16), :].astype(F32)
            mixed = window[14 : 14 + conv_rows] * tap_rows[0:1]
            mixed = mixed + window[15 : 15 + conv_rows] * tap_rows[1:2]
            mixed = mixed + window[16 : 16 + conv_rows] * tap_rows[2:3]
            both[pl.ds(row, conv_rows), local_width:] = (
                proj[GO_, pl.ds(row, conv_rows), :].astype(F32) * mixed
            ).astype(BF16)

    convolve(peer_row)
    acc[...] = jnp.dot(
        both[peer_rows, local_width:], wo[pl.ds(local_width, local_width), :],
        preferred_element_type=F32,
    )
    convolve(my_row)

    start_log = jnp.zeros((heads, BLOCK), F32)
    for i in range(n_sp - 1):
        merged = jnp.maximum(scal_in[i, 0:heads, :] + start_log, scal_in[i, heads : 2 * heads, :])
        start_log = jnp.where(i < me, merged, start_log)
    carried_log = table[T_CARRY] + jnp.concatenate([start_log] * nblocks, axis=0)
    new_top = jnp.maximum(table[T_TOP], carried_log)
    keep = jnp.exp(table[T_TOP] - new_top)
    bring = jnp.exp(carried_log - new_top)
    for b in range(nblocks):
        rows = slice(b * heads, (b + 1) * heads)
        cols[b] = jnp.concatenate([keep[rows], bring[rows], fill], axis=0).T

    wait_from(state_out, state_in, st_s, st_r)

    pieces = 2
    piece_rows = own // pieces

    def finish(row):
        for i in range(piece_rows // BLOCK):
            b = row // BLOCK + i
            rows = pl.ds(pl.multiple_of(b * BLOCK, BLOCK), BLOCK)
            columns = cols[b]
            for h in range(heads):
                hs = slice(h * dh, (h + 1) * dh)
                start = state_in[h * per_head : (h + 1) * per_head].reshape(dh, dh)
                readout = columns[:, h : h + 1] * read[rows, hs] + columns[
                    :, heads + h : heads + h + 1
                ] * jnp.dot(proj[Q_, rows, hs], start, preferred_element_type=F32)
                normalized = readout * lax.rsqrt(
                    jnp.mean(readout * readout, axis=-1, keepdims=True) + EPSILON
                )
                both[rows, hs] = (normalized * sig[rows, hs]).astype(BF16)

    def send_part(i):
        return pltpu.make_async_remote_copy(
            src_ref=part.at[pl.ds(i * piece_rows, piece_rows), :],
            dst_ref=part_in.at[pl.ds(i * piece_rows, piece_rows), :],
            send_sem=out_s.at[i], recv_sem=out_r.at[i],
            device_id={"tp": other}, device_id_type=MESH,
        )

    finish(peer_row)
    for i in range(pieces):
        rows = pl.ds(i * piece_rows, piece_rows)
        if i + 1 < pieces:
            finish(peer_row + (i + 1) * piece_rows)
        else:
            finish(my_row)
        part[rows, :] = (
            acc[rows, :]
            + jnp.dot(
                both[pl.ds(peer_row + i * piece_rows, piece_rows), 0:local_width],
                wo[pl.ds(0, local_width), :],
                preferred_element_type=F32,
            )
        ).astype(BF16)
        send_part(i).start()

    for i in range(pieces):
        if i + 1 < pieces:
            finish(my_row + (i + 1) * piece_rows)
        mine = jnp.dot(
            both[pl.ds(my_row + i * piece_rows, piece_rows), :], wo[...],
            preferred_element_type=F32,
        ).astype(BF16)
        rows = pl.ds(i * piece_rows, piece_rows)
        send_part(i).wait_recv()
        out[0, rows, :] = (mine.astype(F32) + part_in[rows, :].astype(F32)).astype(BF16)

    send_rows.wait_send()
    send_gates.wait_send()
    rim.wait_send()

    def drain(k, carry):
        target = lax.rem(me + k, n_sp)
        for src, send, recv, dst in (
            (scal, scal_s, scal_r, scal_in.at[me]),
            (seg.at[target], seg_s, seg_r, seg_in.at[me]),
            (state_out.at[target], st_s, st_r, state_in.at[me]),
        ):
            pltpu.make_async_remote_copy(
                src_ref=src, dst_ref=dst,
                send_sem=send.at[target], recv_sem=recv.at[me],
                device_id={"sp": target}, device_id_type=MESH,
            ).wait_send()
        return carry

    lax.fori_loop(1, n_sp, drain, 0)
    for i in range(pieces):
        send_part(i).wait_send()


def store_kernel(src, dst, sems):
    rows = src.shape[1] // 4
    copies = [
        pltpu.make_async_copy(
            src.at[0, pl.ds(i * rows, rows), :], dst.at[0, pl.ds(i * rows, rows), :], sems.at[i]
        )
        for i in range(4)
    ]
    for copy in copies:
        copy.start()
    for copy in copies:
        copy.wait()


def local_layer(
    n_sp,
    tokens, norm_gain, w_query, w_key, w_value, w_outgate, w_gatein, w_gateout, w_convin,
    w_igate, w_fgate, input_bias, forget_bias, forget_extra, init_memory, head_gain, conv_taps,
    out_memory, out_conv,
):
    own, width = tokens.shape[1:]
    count = 2 * own
    local_width = w_query.shape[1]
    heads, dh = init_memory.shape[1], init_memory.shape[3]
    nblocks = count // BLOCK
    slice_rows = heads * dh // n_sp
    vmem = pltpu.VMEM
    dma = pltpu.SemaphoreType.DMA
    scratch = [
        vmem((own, width), BF16),
        vmem((width // 128, 128), BF16),
        vmem((count, width), BF16),
        vmem((7, width, local_width), BF16),
        vmem((2 * local_width, width), BF16),
        vmem((2 * heads, width), BF16),
        vmem((2 * heads, width), BF16),
        vmem((7, count, local_width), BF16),
        vmem((4 * heads, count), F32),
        vmem((heads, count), F32),
        vmem((1, 2 * heads), F32),
        vmem((1, 2 * heads), F32),
        vmem(conv_taps.shape, BF16),
        vmem((2 * heads, dh), BF16),
        vmem((slice_rows, dh), F32),
        vmem((nblocks, heads, dh, BLOCK), BF16),
        vmem((nblocks, heads, dh, dh), BF16),
        vmem((6, nblocks * heads, BLOCK), F32),
        vmem((nblocks, BLOCK, BLOCK), F32),
        vmem((nblocks, heads, dh, dh), F32),
        vmem((n_sp, slice_rows, dh), BF16),
        vmem((n_sp, slice_rows, dh), BF16),
        vmem((2 * heads, BLOCK), F32),
        vmem((n_sp, 2 * heads, BLOCK), F32),
        vmem((n_sp, slice_rows, dh), BF16),
        vmem((n_sp, slice_rows, dh), BF16),
        vmem((16, local_width), BF16),
        vmem((count, local_width), F32),
        vmem((count, local_width), F32),
        vmem((count + 16, local_width), BF16),
        vmem((count, 2 * local_width), BF16),
        vmem((own, width), F32),
        vmem((own, width), BF16),
        vmem((own, width), BF16),
        dma((L_W + 7,)),
        dma, dma, dma, dma,
        dma((n_sp,)), dma((n_sp,)),
        dma((n_sp,)), dma((n_sp,)),
        dma((n_sp,)), dma((n_sp,)),
        dma, dma,
        dma((2,)), dma((2,)),
    ]
    rows = pl.pallas_call(
        functools.partial(kernel, n_sp),
        out_shape=vmem(tokens.shape, BF16),
        in_specs=[pl.BlockSpec(memory_space=pl.ANY)] * 19,
        out_specs=pl.BlockSpec(memory_space=pltpu.VMEM),
        scratch_shapes=scratch,
        compiler_params=pltpu.CompilerParams(
            collective_id=0, has_side_effects=True, vmem_limit_bytes=58 * 1024 * 1024
        ),
    )(
        tokens, norm_gain.reshape(-1, 128),
        w_query, w_key, w_value, w_outgate, w_gatein, w_gateout, w_convin,
        w_igate.T, w_fgate.T, input_bias.reshape(1, -1), forget_bias.reshape(1, -1),
        jnp.swapaxes(forget_extra, 1, 2), init_memory, head_gain.reshape(-1, dh), conv_taps,
        out_memory, out_conv,
    )
    return pl.pallas_call(
        store_kernel,
        out_shape=jax.ShapeDtypeStruct(tokens.shape, BF16),
        in_specs=[pl.BlockSpec(memory_space=pltpu.VMEM)],
        out_specs=pl.BlockSpec(memory_space=pl.ANY),
        scratch_shapes=[dma((4,))],
    )(pltpu.with_memory_space_constraint(rows, pltpu.VMEM))


def solution(mesh):
    rows = P("fs", ("sp", "tp"), None)
    column, replicated = P(None, "tp"), P()
    return jax.shard_map(
        functools.partial(local_layer, mesh.shape["sp"]),
        mesh=mesh,
        in_specs=(
            rows, replicated,
            column, column, column, column, column, column, column,
            replicated, replicated, replicated, replicated,
            P("fs", "sp", "tp"), P("fs", "tp", None, None),
            replicated, replicated,
            P("tp", None), P("tp", None),
        ),
        out_specs=rows,
        check_vma=False,
    )
```

time: 58.1 us -> 43.2 us (0.74)
  local copies, waits for them, and re-layouts: 11 us -> 0 us
  Pallas kernels: 46.5 us -> 42.9 us
    unnamed x4 -> x0, local copies, waits for them, and re-layouts: 8.44 us -> none
    pallas_call x1 -> x2, Pallas kernels: 46.5 us -> 42.9 us  [the longest x1 41.6 us: local_layer(): pl.pallas_call(functools.partial(kernel, n_sp), out_shape=vmem(tokens.sha...]
    reshape x2 -> x0, local copies, waits for them, and re-layouts: 2.55 us -> none  [the longest x1 1.29 us: local_layer(): norm_gain.reshape(1, -1)]
where the time goes in v2:
time: 43.2 us; the launch traced here: 43.1 us
  Pallas kernels  42.9 us (99%)
    pallas_call x1, Pallas kernels, local_layer(): pl.pallas_call(functools.partial(kernel, n_sp), out_shape=vmem(tokens.sha...  41.6 us
    pallas_call x1, Pallas kernels, local_layer(): pl.pallas_call(store_kernel, out_shape=jax.ShapeDtypeStruct(tokens.shape,...  1.35 us

profile of v2, /device:TPU:1, one launch (start us, length us, event | category | flops | bytes accessed | tf_op | source)
XLA Modules:
  0.0 43.1 jit_solution(7271000033728532280)
XLA Ops:
  0.0 41.6 %shard_map.181.src = bf16[1,512,2048]{2,1,0:T(8,128)(2,1)S(1)} custom-call(bf16[1,512,2048]{2,1,0:T(8,128)(2,1)} %tokens.1, bf16[16,128]{1,0:T(8,128)(2,1)} %bitcast.10, bf16[2048,512]{1,0:T(8,128)(2,1)} %w_query.1, bf16[2048,512]{1,0:T(8,128)(2,1)} %w_key.1, bf16[2048,512]{1,0:T(8,128)(2,1)} %w_value.1, bf16[2048,512]{1,0:T(8,128)(2,1)} %w_outgate.1, ...), custom_call_target="tpu_custom_call" | custom-call | tf_op jit(solution)/shard_map/pallas_call | solution.py:592
  41.6 1.3 %shard_map.182 = bf16[1,512,2048]{2,1,0:T(8,128)(2,1)} custom-call(bf16[1,512,2048]{2,1,0:T(8,128)(2,1)S(1)} %shard_map.181.src), custom_call_target="tpu_custom_call" | custom-call | tf_op jit(solution)/shard_map/pallas_call | solution.py:608

commit v3 on v2

v3 whole, which is shorter than its diff:
```python
import functools
import math

import jax
import jax.numpy as jnp
from jax import lax
from jax.experimental import pallas as pl
from jax.experimental.pallas import tpu as pltpu
from jax.sharding import PartitionSpec as P

MESH = pl.DeviceIdType.MESH
F32 = jnp.float32
BF16 = jnp.bfloat16
BLOCK = 128
EPSILON = 1e-06
LOWEST_LOG = -1e30

K_, V_, Q_, OG_, GI_, CI_, GO_ = range(7)
T_BIAS, T_KW, T_ALPHA, T_BETA, T_TOP, T_CARRY = range(6)
L_TOK, L_WIG, L_WFG, L_GAIN, L_FE, L_IB, L_FB, L_TAPS, L_HG, L_OM, L_OC, L_INIT, L_W = (
    0, 4, 5, 6, 7, 8, 9, 10, 11, 12, 13, 14, 16,
)


def kernel(
    n_sp,
    tokens, norm_gain, w_query, w_key, w_value, w_outgate, w_gatein, w_gateout, w_convin,
    w_igate, w_fgate, input_bias, forget_bias, forget_extra, init_memory, head_gain, conv_taps,
    out_memory, out_conv,
    out,
    tok, gain, w_all, wom, woc, wig, wfg, gates, fe, ib, fb, taps, hg, init,
    x_own, x_peer, proj_own, proj_peer, sig_own, sig_peer, read_own, read_peer,
    conv_own, conv_peer, conv_in, acc, mem_0, mem_1, mem_2, mem_3, mem_in, wom_in, woc_in,
    keys, table, cols, cols_in, terms, seg, seg_in, scal, scal_in, state_out, state_in,
    rim_in, prod,
    ready, lsem, tok_s, tok_r, gate_s, gate_r, seg_s, seg_r, scal_s, scal_r, st_s, st_r,
    rim_s, rim_r, ow_s, ow_r, conv_s, conv_r, mem_s, mem_r,
):
    own = tokens.shape[1]
    count = 2 * own
    local_width = w_query.shape[1]
    heads = init_memory.shape[1]
    dh = init_memory.shape[3]
    nblocks = count // BLOCK
    half_blocks = nblocks // 2
    slice_rows = heads * dh // n_sp
    per_head = dh // slice_rows
    key_log = -0.5 * math.log(dh)
    me = lax.axis_index("sp")
    side = lax.axis_index("tp")
    other = 1 - side
    my_row = pl.multiple_of(side * own, own)
    peer_row = pl.multiple_of(other * own, own)
    my_block = side * half_blocks
    peer_block = other * half_blocks
    my_head = (me * slice_rows) // dh
    my_depth = pl.multiple_of(me * slice_rows - my_head * dh, slice_rows)
    my_lane = pl.multiple_of(side * local_width, local_width)
    my_rows = pl.ds(my_row, own)
    peer_rows = pl.ds(peer_row, own)

    def local(src, dst, index):
        return pltpu.make_async_copy(src, dst, lsem.at[index])

    def sp(target):
        return dict(device_id={"sp": target}, device_id_type=MESH)

    peer = dict(device_id={"tp": other}, device_id_type=MESH)
    weights = (w_key, w_value, w_query, w_outgate, w_gatein, w_convin, w_gateout)

    barrier = pltpu.get_barrier_semaphore()
    chunks = 4
    chunk_rows = own // chunks
    token_copies = [
        local(
            tokens.at[0, pl.ds(c * chunk_rows, chunk_rows), :],
            tok.at[pl.ds(c * chunk_rows, chunk_rows), :],
            L_TOK + c,
        )
        for c in range(chunks)
    ]
    gain_copy = local(norm_gain, gain, L_GAIN)
    narrow_copies = [local(w_igate, wig, L_WIG), local(w_fgate, wfg, L_WFG)]
    w_copies = [local(weights[p], w_all[p], L_W + p) for p in range(7)]
    gate_copies = [
        local(forget_extra.at[0], fe, L_FE),
        local(input_bias, ib, L_IB),
        local(forget_bias, fb, L_FB),
    ]
    head_copy = local(head_gain, hg, L_HG)
    taps_copy = local(conv_taps, taps, L_TAPS)
    init_copy = local(init_memory.at[0, my_head, pl.ds(my_depth, slice_rows), :], init, L_INIT)
    out_copies = [local(out_conv, woc, L_OC), local(out_memory, wom, L_OM)]
    gain_copy.start()
    for copy in token_copies + narrow_copies + w_copies[:2] + gate_copies:
        copy.start()
    pl.semaphore_signal(barrier, inc=1, **peer)

    def greet(k, carry):
        pl.semaphore_signal(barrier, inc=1, **sp(k))
        return carry

    lax.fori_loop(me + 1, n_sp, greet, 0)

    gain_copy.wait()
    gain_row = jnp.concatenate(
        [gain[i : i + 1, :] for i in range(gain.shape[0])], axis=1
    ).astype(F32)
    step_rows = 64
    for c in range(chunks):
        token_copies[c].wait()

        def norm_step(i, carry):
            rows = pl.ds(pl.multiple_of(c * chunk_rows + i * step_rows, step_rows), step_rows)
            values = tok[rows, :].astype(F32)
            scale = lax.rsqrt(jnp.mean(values * values, axis=-1, keepdims=True) + EPSILON)
            x_own[rows, :] = (values * scale * gain_row).astype(BF16)
            return carry

        lax.fori_loop(0, chunk_rows // step_rows, norm_step, 0)

    for copy in narrow_copies:
        copy.wait()
    narrow = jnp.concatenate([wig[...], wfg[...]], axis=0)
    gates[:, my_rows] = lax.dot_general(
        narrow, x_own[...], (((1,), (1,)), ((), ())), preferred_element_type=F32
    )

    pl.semaphore_wait(barrier, me + 1)
    send_rows = pltpu.make_async_remote_copy(
        src_ref=x_own, dst_ref=x_peer, send_sem=tok_s, recv_sem=tok_r, **peer
    )
    send_gates = pltpu.make_async_remote_copy(
        src_ref=gates.at[:, my_rows], dst_ref=gates.at[:, my_rows],
        send_sem=gate_s, recv_sem=gate_r, **peer,
    )
    take_gates = pltpu.make_async_remote_copy(
        src_ref=gates.at[:, peer_rows], dst_ref=gates.at[:, peer_rows],
        send_sem=gate_s, recv_sem=gate_r, **peer,
    )
    send_gates.start()
    send_rows.start()

    def answer(k, carry):
        pl.semaphore_signal(ready, inc=1, **sp(k))
        return carry

    lax.fori_loop(0, me, answer, 0)

    pieces = 2
    piece_rows = own // pieces
    spans = [slice(i * piece_rows, (i + 1) * piece_rows) for i in range(pieces)]

    def project(p, rows, dst):
        for at in spans:
            dst[p][at, :] = jnp.dot(
                rows[at, :], w_all[p][...], preferred_element_type=F32
            ).astype(BF16)

    def head_gains():
        gains = hg[...].astype(F32)
        gains = jnp.where(side == 0, gains[0:heads], gains[heads : 2 * heads])
        return jnp.concatenate([gains[i : i + 1] for i in range(heads)], axis=1)

    def project_sig(rows, dst):
        head_row = head_gains()
        for at in spans:
            value = jnp.dot(
                rows[at, :], w_all[OG_][...], preferred_element_type=F32
            ).astype(BF16)
            dst[at, :] = head_row * jax.nn.sigmoid(value.astype(F32))

    def piece_of(p, rows, dst, i):
        at = spans[i]
        dst[p][at, :] = jnp.dot(
            rows[at, :], w_all[p][...], preferred_element_type=F32
        ).astype(BF16)

    def prod_piece(rows, proj, row, i):
        at = spans[i]
        value = jnp.dot(rows[at, :], w_all[CI_][...], preferred_element_type=F32).astype(BF16)
        prod[pl.ds(row + 16 + i * piece_rows, piece_rows), :] = (
            proj[GI_][at, :].astype(F32) * value.astype(F32)
        ).astype(BF16)

    w_copies[K_].wait()
    w_copies[V_].wait()
    for copy in w_copies[2:4] + [head_copy] + w_copies[4:]:
        copy.start()
    for copy in [taps_copy, init_copy] + out_copies:
        copy.start()
    project(K_, x_own, proj_own)
    project(V_, x_own, proj_own)
    w_copies[Q_].wait()
    w_copies[OG_].wait()
    head_copy.wait()
    for copy in gate_copies:
        copy.wait()
    take_gates.wait_recv()

    lanes = lax.broadcasted_iota(jnp.int32, (nblocks * heads, BLOCK), 1)
    head_rows = lax.broadcasted_iota(jnp.int32, (heads, BLOCK), 0)
    bias_in = jnp.zeros((heads, BLOCK), F32)
    bias_forget = jnp.zeros((heads, BLOCK), F32)
    for h in range(heads):
        for part_index in range(2):
            pick = (head_rows == h) & (side == part_index)
            c = part_index * heads + h
            bias_in = jnp.where(pick, ib[0:1, c : c + 1], bias_in)
            bias_forget = jnp.where(pick, fb[0:1, c : c + 1], bias_forget)
    ins, forgets = [], []
    for b in range(nblocks):
        at = slice(b * BLOCK, (b + 1) * BLOCK)
        pre = gates[:, at]
        ins.append(jnp.where(side == 0, pre[0:heads], pre[heads : 2 * heads]) + bias_in)
        forget = (
            jnp.where(side == 0, pre[2 * heads : 3 * heads], pre[3 * heads : 4 * heads])
            + bias_forget
        )
        forgets.append(
            jnp.minimum(forget, 0.0) - jnp.log1p(jnp.exp(-jnp.abs(forget))) + fe[:, at]
        )
    ins = jnp.concatenate(ins, axis=0)
    cumulative = jnp.concatenate(forgets, axis=0)
    shift = 1
    while shift < BLOCK:
        cumulative = cumulative + jnp.where(
            lanes >= shift, pltpu.roll(cumulative, shift, 1), 0.0
        )
        shift *= 2
    pair = ins - cumulative
    top = pair
    shift = 1
    while shift < BLOCK:
        top = jnp.maximum(top, jnp.where(lanes >= shift, pltpu.roll(top, shift, 1), top))
        shift *= 2
    total = jnp.broadcast_to(cumulative[:, BLOCK - 1 :], cumulative.shape)
    last_top = jnp.broadcast_to(top[:, BLOCK - 1 :], top.shape)
    log_scale = jnp.full((heads, BLOCK), LOWEST_LOG, F32)
    before = jnp.zeros((heads, BLOCK), F32)
    scales, befores, alphas, betas = [], [], [], []
    for b in range(nblocks):
        block_total = total[b * heads : (b + 1) * heads]
        block_top = block_total + last_top[b * heads : (b + 1) * heads]
        scales.append(log_scale)
        befores.append(before)
        merged = jnp.maximum(block_total + log_scale, block_top)
        alphas.append(block_total + log_scale - merged)
        betas.append(block_top - merged)
        log_scale = merged
        before = before + block_total
    scal[0:heads, :] = before
    scal[heads : 2 * heads, :] = log_scale
    scal_in[me] = scal[...]
    scales = jnp.concatenate(scales, axis=0)
    row_top = jnp.maximum(scales, top)
    table[T_BIAS] = pair + key_log
    table[T_KW] = jnp.exp(pair + key_log - last_top)
    table[T_ALPHA] = jnp.exp(jnp.concatenate(alphas, axis=0))
    table[T_BETA] = jnp.exp(jnp.concatenate(betas, axis=0))
    table[T_TOP] = row_top
    table[T_CARRY] = jnp.concatenate(befores, axis=0)
    carry_weight = jnp.exp(scales - row_top)
    fill = jnp.zeros((BLOCK - 2 * heads, BLOCK), F32)
    for b in range(nblocks):
        rows = slice(b * heads, (b + 1) * heads)
        cols[b] = jnp.concatenate([row_top[rows], carry_weight[rows], fill], axis=0).T
    project(Q_, x_own, proj_own)
    project_sig(x_own, sig_own)

    def weigh_keys(proj, first):
        weighted = []
        for i in range(half_blocks):
            rows = slice(i * BLOCK, (i + 1) * BLOCK)
            b = first + i
            for h in range(heads):
                turned = proj[K_][rows, h * dh : (h + 1) * dh].T
                keys[b, h, :, 0:BLOCK] = turned
                weighted.append(
                    (turned.astype(F32) * table[T_KW, pl.ds(b * heads + h, 1), :]).astype(BF16)
                )
        return weighted

    def block_terms(weighted, proj, first):
        for i in range(half_blocks):
            rows = slice(i * BLOCK, (i + 1) * BLOCK)
            for h in range(heads):
                terms[first + i, h] = jnp.dot(
                    weighted[i * heads + h], proj[V_][rows, h * dh : (h + 1) * dh],
                    preferred_element_type=F32,
                )

    w_copies[GI_].wait()
    w_copies[CI_].wait()
    w_copies[GO_].wait()
    take_rows = pltpu.make_async_remote_copy(
        src_ref=x_own, dst_ref=x_peer, send_sem=tok_s, recv_sem=tok_r, **peer
    )
    take_rows.wait_recv()
    out_weights = [
        pltpu.make_async_remote_copy(
            src_ref=src, dst_ref=dst, send_sem=ow_s.at[i], recv_sem=ow_r.at[i], **peer
        )
        for i, (src, dst) in enumerate(((out_conv, woc_in), (out_memory, wom_in)))
    ]
    for copy in out_weights:
        copy.start()
    weighted_own = weigh_keys(proj_own, my_block)
    project(K_, x_peer, proj_peer)
    block_terms(weighted_own, proj_own, my_block)
    weighted_peer = weigh_keys(proj_peer, peer_block)
    project(V_, x_peer, proj_peer)
    block_terms(weighted_peer, proj_peer, peer_block)

    @pl.when(me < n_sp - 1)
    def _():
        pl.semaphore_wait(ready, n_sp - 1 - me)

    for h in range(heads):
        held = jnp.zeros((dh, dh), F32)
        for b in range(nblocks):
            at = pl.ds(b * heads + h, 1)
            keys[b, h, :, BLOCK:] = held.astype(BF16)
            held = table[T_ALPHA, at, :] * held + table[T_BETA, at, :] * terms[b, h]
        for piece in range(per_head):
            seg[h * per_head + piece] = held[
                piece * slice_rows : (piece + 1) * slice_rows, :
            ].astype(BF16)
    seg_in[me] = seg[me]

    def segment_copies(target):
        return (
            pltpu.make_async_remote_copy(
                src_ref=scal, dst_ref=scal_in.at[me],
                send_sem=scal_s.at[target], recv_sem=scal_r.at[me], **sp(target),
            ),
            pltpu.make_async_remote_copy(
                src_ref=seg.at[target], dst_ref=seg_in.at[me],
                send_sem=seg_s.at[target], recv_sem=seg_r.at[me], **sp(target),
            ),
        )

    for k in range(1, n_sp):
        for copy in segment_copies(lax.rem(me + k, n_sp)):
            copy.start()
    project(GI_, x_own, proj_own)

    t_index = lax.broadcasted_iota(jnp.int32, (BLOCK, BLOCK), 0)
    s_index = lax.broadcasted_iota(jnp.int32, (BLOCK, BLOCK), 1)
    causal = s_index <= t_index

    def read_blocks(proj, read, first, chunks):
        def scores_of(i):
            rows = slice(i * BLOCK, (i + 1) * BLOCK)
            return [
                jnp.dot(
                    proj[Q_][rows, h * dh : (h + 1) * dh], keys[first + i, h],
                    preferred_element_type=F32,
                )
                for h in range(heads)
            ]

        def weigh(i, raw):
            columns = cols[first + i]
            weighted, carried = [], []
            for h in range(heads):
                log_weight = jnp.where(
                    causal,
                    table[T_BIAS, pl.ds((first + i) * heads + h, 1), :] - columns[:, h : h + 1],
                    -jnp.inf,
                )
                weighted.append((jnp.exp(log_weight) * raw[h][:, 0:BLOCK]).astype(BF16))
                carried.append(columns[:, heads + h : heads + h + 1] * raw[h][:, BLOCK:])
            return weighted, carried

        def read_out(i, weighted, carried):
            rows = slice(i * BLOCK, (i + 1) * BLOCK)
            for h in range(heads):
                hs = slice(h * dh, (h + 1) * dh)
                read[rows, hs] = carried[h] + jnp.dot(
                    weighted[h], proj[V_][rows, hs], preferred_element_type=F32
                )

        raw = scores_of(0)
        for i in range(half_blocks):
            parts = weigh(i, raw)
            chunks[i]()
            if i + 1 < half_blocks:
                raw = scores_of(i + 1)
            read_out(i, *parts)
        for chunk in chunks[half_blocks:]:
            chunk()

    read_blocks(
        proj_own, read_own, my_block,
        [
            lambda: prod_piece(x_own, proj_own, my_row, 0),
            lambda: prod_piece(x_own, proj_own, my_row, 1),
            lambda: piece_of(GI_, x_peer, proj_peer, 0),
            lambda: piece_of(GI_, x_peer, proj_peer, 1),
        ],
    )
    project(Q_, x_peer, proj_peer)

    def owner_step():
        init_copy.wait()

        def wait_segment(k, carry):
            source = lax.rem(me + k, n_sp)
            pltpu.make_async_remote_copy(
                src_ref=scal, dst_ref=scal_in.at[source],
                send_sem=scal_s.at[source], recv_sem=scal_r.at[source], **sp(source),
            ).wait_recv()
            pltpu.make_async_remote_copy(
                src_ref=seg.at[source], dst_ref=seg_in.at[source],
                send_sem=seg_s.at[source], recv_sem=seg_r.at[source], **sp(source),
            ).wait_recv()
            return carry

        lax.fori_loop(1, n_sp, wait_segment, 0)
        state = init[...]
        state_log = jnp.zeros((1, BLOCK), F32)
        for i in range(n_sp):
            state_out[i] = state.astype(BF16)
            if i == n_sp - 1:
                break
            span = scal_in[i, pl.ds(my_head, 1), :]
            span_top = scal_in[i, pl.ds(heads + my_head, 1), :]
            merged = jnp.maximum(span + state_log, span_top)
            state = (
                jnp.exp(span + state_log - merged) * state
                + jnp.exp(span_top - merged) * seg_in[i].astype(F32)
            )
            state_log = merged
        state_in[me] = state_out[me]

        def send_state(k, carry):
            target = lax.rem(me + k, n_sp)
            pltpu.make_async_remote_copy(
                src_ref=state_out.at[target], dst_ref=state_in.at[me],
                send_sem=st_s.at[target], recv_sem=st_r.at[me], **sp(target),
            ).start()
            return carry

        lax.fori_loop(1, n_sp, send_state, 0)

    along_x, along_z = lax.rem(me, 4), me // 4
    lateness = 2 * along_z + jnp.where(along_x == 3, 3, 2 * along_x)
    late = lateness >= 6
    early = lateness < 4
    pl.when(late)(owner_step)

    prod_piece(x_peer, proj_peer, peer_row, 0)
    prod_piece(x_peer, proj_peer, peer_row, 1)

    def rim_copy(target):
        return pltpu.make_async_remote_copy(
            src_ref=prod.at[pl.ds(count, 16), :], dst_ref=rim_in,
            send_sem=rim_s, recv_sem=rim_r, **sp(target),
        )

    last = me == n_sp - 1

    @pl.when(jnp.logical_not(last))
    def _():
        rim_copy(me + 1).start()

    pl.when(jnp.logical_not(late | early))(owner_step)

    read_blocks(
        proj_peer, read_peer, peer_block,
        [
            lambda: piece_of(GO_, x_own, proj_own, 0),
            lambda: piece_of(GO_, x_own, proj_own, 1),
            lambda: piece_of(GO_, x_peer, proj_peer, 0),
            lambda: piece_of(GO_, x_peer, proj_peer, 1),
        ],
    )

    pl.when(early)(owner_step)

    taps_copy.wait()
    for copy in out_copies:
        copy.wait()

    @pl.when(me == 0)
    def _():
        rim_in[...] = jnp.zeros_like(rim_in)

    @pl.when(me > 0)
    def _():
        rim_copy(me - 1).wait_recv()

    prod[0:16, :] = rim_in[...]
    tap_rows = taps[:, pl.ds(my_lane, local_width)].astype(F32)
    conv_rows = 64

    def convolve(proj, dst, first):
        for i in range(own // conv_rows):
            row = pl.multiple_of(first + i * conv_rows, conv_rows)
            rows = slice(i * conv_rows, (i + 1) * conv_rows)
            window = prod[pl.ds(row, conv_rows + 16), :].astype(F32)
            mixed = window[14 : 14 + conv_rows] * tap_rows[0:1]
            mixed = mixed + window[15 : 15 + conv_rows] * tap_rows[1:2]
            mixed = mixed + window[16 : 16 + conv_rows] * tap_rows[2:3]
            dst[rows, :] = (proj[GO_][rows, :].astype(F32) * mixed).astype(BF16)

    convolve(proj_peer, conv_peer, peer_row)
    send_conv = pltpu.make_async_remote_copy(
        src_ref=conv_peer, dst_ref=conv_in, send_sem=conv_s, recv_sem=conv_r, **peer
    )
    project_sig(x_peer, sig_peer)
    send_conv.start()
    convolve(proj_own, conv_own, my_row)
    start_log = jnp.zeros((heads, BLOCK), F32)
    for i in range(n_sp - 1):
        merged = jnp.maximum(scal_in[i, 0:heads, :] + start_log, scal_in[i, heads : 2 * heads, :])
        start_log = jnp.where(i < me, merged, start_log)
    carried_log = table[T_CARRY] + jnp.concatenate([start_log] * nblocks, axis=0)
    new_top = jnp.maximum(table[T_TOP], carried_log)
    keep = jnp.exp(table[T_TOP] - new_top)
    bring = jnp.exp(carried_log - new_top)
    for b in range(nblocks):
        rows = slice(b * heads, (b + 1) * heads)
        cols_in[b] = jnp.concatenate([keep[rows], bring[rows], fill], axis=0).T
    acc[...] = jnp.dot(conv_own[...], woc[...], preferred_element_type=F32)

    def wait_state(k, carry):
        source = lax.rem(me + k, n_sp)
        pltpu.make_async_remote_copy(
            src_ref=state_out.at[source], dst_ref=state_in.at[source],
            send_sem=st_s.at[source], recv_sem=st_r.at[source], **sp(source),
        ).wait_recv()
        return carry

    lax.fori_loop(1, n_sp, wait_state, 0)
    send_conv.wait_recv()
    for copy in out_weights:
        copy.wait_recv()

    piece_blocks = piece_rows // BLOCK

    def bring_in(proj, piece):
        return [
            [
                jnp.dot(
                    proj[Q_][block * BLOCK : (block + 1) * BLOCK, h * dh : (h + 1) * dh],
                    state_in[h * per_head : (h + 1) * per_head].reshape(dh, dh),
                    preferred_element_type=F32,
                )
                for h in range(heads)
            ]
            for block in range(piece * piece_blocks, (piece + 1) * piece_blocks)
        ]

    def finish(brought, read, sig, dst, piece, first):
        for i in range(piece_blocks):
            block = piece * piece_blocks + i
            rows = slice(block * BLOCK, (block + 1) * BLOCK)
            columns = cols_in[first + block]
            for h in range(heads):
                hs = slice(h * dh, (h + 1) * dh)
                readout = (
                    columns[:, h : h + 1] * read[rows, hs]
                    + columns[:, heads + h : heads + h + 1] * brought[i][h]
                )
                normalized = readout * lax.rsqrt(
                    jnp.mean(readout * readout, axis=-1, keepdims=True) + EPSILON
                )
                dst[i * BLOCK : (i + 1) * BLOCK, hs] = (normalized * sig[rows, hs]).astype(BF16)

    def send_memory(i, mem):
        return pltpu.make_async_remote_copy(
            src_ref=mem, dst_ref=mem_in.at[i], send_sem=mem_s.at[i], recv_sem=mem_r.at[i], **peer
        )

    def add_part(at, rows, weight):
        acc[at, :] = acc[at, :] + jnp.dot(rows, weight[...], preferred_element_type=F32)

    brought_0 = bring_in(proj_peer, 0)
    brought_1 = bring_in(proj_peer, 1)
    finish(brought_0, read_peer, sig_peer, mem_0, 0, peer_block)
    send_memory(0, mem_0).start()
    add_part(spans[0], conv_in[spans[0], :], woc_in)
    finish(brought_1, read_peer, sig_peer, mem_1, 1, peer_block)
    send_memory(1, mem_1).start()
    brought_2 = bring_in(proj_own, 0)
    finish(brought_2, read_own, sig_own, mem_2, 0, my_block)
    add_part(spans[1], conv_in[spans[1], :], woc_in)
    brought_3 = bring_in(proj_own, 1)
    finish(brought_3, read_own, sig_own, mem_3, 1, my_block)
    add_part(spans[0], mem_2[...], wom)
    add_part(spans[1], mem_3[...], wom)

    for i, at in enumerate(spans):
        send_memory(i, (mem_0, mem_1)[i]).wait_recv()
    for i, at in enumerate(spans):
        out[0, at, :] = (
            acc[at, :] + jnp.dot(mem_in[i], wom_in[...], preferred_element_type=F32)
        ).astype(BF16)

    send_rows.wait_send()
    send_gates.wait_send()

    @pl.when(jnp.logical_not(last))
    def _():
        rim_copy(me + 1).wait_send()

    def drain(k, carry):
        target = lax.rem(me + k, n_sp)
        for copy in segment_copies(target):
            copy.wait_send()
        pltpu.make_async_remote_copy(
            src_ref=state_out.at[target], dst_ref=state_in.at[me],
            send_sem=st_s.at[target], recv_sem=st_r.at[me], **sp(target),
        ).wait_send()
        return carry

    lax.fori_loop(1, n_sp, drain, 0)
    send_conv.wait_send()
    for copy in out_weights:
        copy.wait_send()
    for i, mem in enumerate((mem_0, mem_1)):
        send_memory(i, mem).wait_send()


def store_kernel(src, dst, sems):
    rows = src.shape[1] // 4
    copies = [
        pltpu.make_async_copy(
            src.at[0, pl.ds(i * rows, rows), :], dst.at[0, pl.ds(i * rows, rows), :], sems.at[i]
        )
        for i in range(4)
    ]
    for copy in copies:
        copy.start()
    for copy in copies:
        copy.wait()


def local_layer(
    n_sp,
    tokens, norm_gain, w_query, w_key, w_value, w_outgate, w_gatein, w_gateout, w_convin,
    w_igate, w_fgate, input_bias, forget_bias, forget_extra, init_memory, head_gain, conv_taps,
    out_memory, out_conv,
):
    own, width = tokens.shape[1:]
    count = 2 * own
    local_width = w_query.shape[1]
    heads, dh = init_memory.shape[1], init_memory.shape[3]
    nblocks = count // BLOCK
    slice_rows = heads * dh // n_sp
    vmem = pltpu.VMEM
    dma = pltpu.SemaphoreType.DMA
    half = vmem((own, local_width), BF16)
    half_wide = vmem((own, local_width), F32)
    quarter = vmem((own // 2, local_width), BF16)
    scratch = [
        vmem((own, width), BF16),
        vmem((width // 128, 128), BF16),
        [vmem((width, local_width), BF16)] * 7,
        vmem((local_width, width), BF16),
        vmem((local_width, width), BF16),
        vmem((2 * heads, width), BF16),
        vmem((2 * heads, width), BF16),
        vmem((4 * heads, count), F32),
        vmem((heads, count), F32),
        vmem((1, 2 * heads), F32),
        vmem((1, 2 * heads), F32),
        vmem(conv_taps.shape, BF16),
        vmem((2 * heads, dh), BF16),
        vmem((slice_rows, dh), F32),
        vmem((own, width), BF16),
        vmem((own, width), BF16),
        [half] * 7,
        [half] * 7,
        half_wide, half_wide,
        half_wide, half_wide,
        half, half, half,
        vmem((own, width), F32),
        quarter, quarter, quarter, quarter,
        vmem((2, own // 2, local_width), BF16),
        vmem((local_width, width), BF16),
        vmem((local_width, width), BF16),
        vmem((nblocks, heads, dh, 2 * BLOCK), BF16),
        vmem((6, nblocks * heads, BLOCK), F32),
        vmem((nblocks, BLOCK, BLOCK), F32),
        vmem((nblocks, BLOCK, BLOCK), F32),
        vmem((nblocks, heads, dh, dh), F32),
        vmem((n_sp, slice_rows, dh), BF16),
        vmem((n_sp, slice_rows, dh), BF16),
        vmem((2 * heads, BLOCK), F32),
        vmem((n_sp, 2 * heads, BLOCK), F32),
        vmem((n_sp, slice_rows, dh), BF16),
        vmem((n_sp, slice_rows, dh), BF16),
        vmem((16, local_width), BF16),
        vmem((count + 16, local_width), BF16),
        pltpu.SemaphoreType.REGULAR,
        dma((L_W + 7,)),
        dma, dma, dma, dma,
        dma((n_sp,)), dma((n_sp,)),
        dma((n_sp,)), dma((n_sp,)),
        dma((n_sp,)), dma((n_sp,)),
        dma, dma,
        dma((2,)), dma((2,)),
        dma, dma,
        dma((2,)), dma((2,)),
    ]
    rows = pl.pallas_call(
        functools.partial(kernel, n_sp),
        out_shape=vmem(tokens.shape, BF16),
        in_specs=[pl.BlockSpec(memory_space=pl.ANY)] * 19,
        out_specs=pl.BlockSpec(memory_space=pltpu.VMEM),
        scratch_shapes=scratch,
        compiler_params=pltpu.CompilerParams(
            collective_id=0, has_side_effects=True, vmem_limit_bytes=58 * 1024 * 1024
        ),
    )(
        tokens, norm_gain.reshape(-1, 128),
        w_query, w_key, w_value, w_outgate, w_gatein, w_gateout, w_convin,
        w_igate.T, w_fgate.T, input_bias.reshape(1, -1), forget_bias.reshape(1, -1),
        jnp.swapaxes(forget_extra, 1, 2), init_memory, head_gain.reshape(-1, dh), conv_taps,
        out_memory, out_conv,
    )
    return pl.pallas_call(
        store_kernel,
        out_shape=jax.ShapeDtypeStruct(tokens.shape, BF16),
        in_specs=[pl.BlockSpec(memory_space=pltpu.VMEM)],
        out_specs=pl.BlockSpec(memory_space=pl.ANY),
        scratch_shapes=[dma((4,))],
    )(pltpu.with_memory_space_constraint(rows, pltpu.VMEM))


def solution(mesh):
    rows = P("fs", ("sp", "tp"), None)
    column, replicated = P(None, "tp"), P()
    return jax.shard_map(
        functools.partial(local_layer, mesh.shape["sp"]),
        mesh=mesh,
        in_specs=(
            rows, replicated,
            column, column, column, column, column, column, column,
            replicated, replicated, replicated, replicated,
            P("fs", "sp", "tp"), P("fs", "tp", None, None),
            replicated, replicated,
            P("tp", None), P("tp", None),
        ),
        out_specs=rows,
        check_vma=False,
    )
```

time: 43.2 us -> 34.8 us (0.81); the launches traced: 43.1 us -> 34.2 us
  Pallas kernels: 42.9 us -> 34.1 us
    pallas_call x1, Pallas kernels: 41.6 us -> 32.7 us  [local_layer(): pl.pallas_call(functools.partial(kernel, n_sp), out_shape=vmem(tokens.sha...]
where the time goes in v3:
time: 34.8 us; the launch traced here: 34.2 us
  Pallas kernels  34.1 us (98%)
    pallas_call x1, Pallas kernels, local_layer(): pl.pallas_call(functools.partial(kernel, n_sp), out_shape=vmem(tokens.sha...  32.7 us
    pallas_call x1, Pallas kernels, local_layer(): pl.pallas_call(store_kernel, out_shape=jax.ShapeDtypeStruct(tokens.shape,...  1.35 us

profile of v3, /device:TPU:1, one launch (start us, length us, event | category | flops | bytes accessed | tf_op | source)
XLA Modules:
  0.0 34.2 jit_solution(16575669850678022278)
XLA Ops:
  0.0 32.7 %shard_map.181.src = bf16[1,512,2048]{2,1,0:T(8,128)(2,1)S(1)} custom-call(bf16[1,512,2048]{2,1,0:T(8,128)(2,1)} %tokens.1, bf16[16,128]{1,0:T(8,128)(2,1)} %bitcast.10, bf16[2048,512]{1,0:T(8,128)(2,1)} %w_query.1, bf16[2048,512]{1,0:T(8,128)(2,1)} %w_key.1, bf16[2048,512]{1,0:T(8,128)(2,1)} %w_value.1, bf16[2048,512]{1,0:T(8,128)(2,1)} %w_outgate.1, ...), custom_call_target="tpu_custom_call" | custom-call | tf_op jit(solution)/shard_map/pallas_call | solution.py:709
  32.7 1.3 %shard_map.182 = bf16[1,512,2048]{2,1,0:T(8,128)(2,1)} custom-call(bf16[1,512,2048]{2,1,0:T(8,128)(2,1)S(1)} %shard_map.181.src), custom_call_target="tpu_custom_call" | custom-call | tf_op jit(solution)/shard_map/pallas_call | solution.py:725

commit v4 on v3

--- a/solution.py
+++ b/solution.py
@@ -27,10 +27,10 @@
     tokens, norm_gain, w_query, w_key, w_value, w_outgate, w_gatein, w_gateout, w_convin,
     w_igate, w_fgate, input_bias, forget_bias, forget_extra, init_memory, head_gain, conv_taps,
     out_memory, out_conv,
-    out,
+    acc, mem_in, wom_in,
     tok, gain, w_all, wom, woc, wig, wfg, gates, fe, ib, fb, taps, hg, init,
     x_own, x_peer, proj_own, proj_peer, sig_own, sig_peer, read_own, read_peer,
-    conv_own, conv_peer, conv_in, acc, mem_0, mem_1, mem_2, mem_3, mem_in, wom_in, woc_in,
+    conv_own, conv_peer, conv_in, mem_0, mem_1, mem_2, mem_3, woc_in,
     keys, table, cols, cols_in, terms, seg, seg_in, scal, scal_in, state_out, state_in,
     rim_in, prod,
     ready, lsem, tok_s, tok_r, gate_s, gate_r, seg_s, seg_r, scal_s, scal_r, st_s, st_r,
@@ -106,25 +106,28 @@
     gain_row = jnp.concatenate(
         [gain[i : i + 1, :] for i in range(gain.shape[0])], axis=1
     ).astype(F32)
-    step_rows = 64
+    norm_rows = 16
+
+    def own_gates(c):
+        rows = x_own[c * chunk_rows : (c + 1) * chunk_rows, :]
+        gates[:, pl.ds(my_row + c * chunk_rows, chunk_rows)] = lax.dot_general(
+            narrow, rows, (((1,), (1,)), ((), ())), preferred_element_type=F32
+        )
+
     for c in range(chunks):
         token_copies[c].wait()
-
-        def norm_step(i, carry):
-            rows = pl.ds(pl.multiple_of(c * chunk_rows + i * step_rows, step_rows), step_rows)
+        if c == 1:
+            for copy in narrow_copies:
+                copy.wait()
+            narrow = jnp.concatenate([wig[...], wfg[...]], axis=0)
+        if c > 0:
+            own_gates(c - 1)
+        for start in range(c * chunk_rows, (c + 1) * chunk_rows, norm_rows):
+            rows = slice(start, start + norm_rows)
             values = tok[rows, :].astype(F32)
             scale = lax.rsqrt(jnp.mean(values * values, axis=-1, keepdims=True) + EPSILON)
             x_own[rows, :] = (values * scale * gain_row).astype(BF16)
-            return carry
-
-        lax.fori_loop(0, chunk_rows // step_rows, norm_step, 0)
-
-    for copy in narrow_copies:
-        copy.wait()
-    narrow = jnp.concatenate([wig[...], wfg[...]], axis=0)
-    gates[:, my_rows] = lax.dot_general(
-        narrow, x_own[...], (((1,), (1,)), ((), ())), preferred_element_type=F32
-    )
+    own_gates(chunks - 1)
 
     pl.semaphore_wait(barrier, me + 1)
     send_rows = pltpu.make_async_remote_copy(
@@ -162,13 +165,10 @@
         gains = jnp.where(side == 0, gains[0:heads], gains[heads : 2 * heads])
         return jnp.concatenate([gains[i : i + 1] for i in range(heads)], axis=1)
 
-    def project_sig(rows, dst):
-        head_row = head_gains()
-        for at in spans:
-            value = jnp.dot(
-                rows[at, :], w_all[OG_][...], preferred_element_type=F32
-            ).astype(BF16)
-            dst[at, :] = head_row * jax.nn.sigmoid(value.astype(F32))
+    def sig_piece(rows, dst, i):
+        at = spans[i]
+        value = jnp.dot(rows[at, :], w_all[OG_][...], preferred_element_type=F32).astype(BF16)
+        dst[at, :] = head_gains() * jax.nn.sigmoid(value.astype(F32))
 
     def piece_of(p, rows, dst, i):
         at = spans[i]
@@ -266,7 +266,8 @@
         rows = slice(b * heads, (b + 1) * heads)
         cols[b] = jnp.concatenate([row_top[rows], carry_weight[rows], fill], axis=0).T
     project(Q_, x_own, proj_own)
-    project_sig(x_own, sig_own)
+    sig_piece(x_own, sig_own, 0)
+    sig_piece(x_own, sig_own, 1)
 
     def weigh_keys(proj, first):
         weighted = []
@@ -316,6 +317,7 @@
     def _():
         pl.semaphore_wait(ready, n_sp - 1 - me)
 
+    piece_of(GI_, x_own, proj_own, 0)
     for h in range(heads):
         held = jnp.zeros((dh, dh), F32)
         for b in range(nblocks):
@@ -343,13 +345,13 @@
     for k in range(1, n_sp):
         for copy in segment_copies(lax.rem(me + k, n_sp)):
             copy.start()
-    project(GI_, x_own, proj_own)
+    piece_of(GI_, x_own, proj_own, 1)
 
     t_index = lax.broadcasted_iota(jnp.int32, (BLOCK, BLOCK), 0)
     s_index = lax.broadcasted_iota(jnp.int32, (BLOCK, BLOCK), 1)
     causal = s_index <= t_index
 
-    def read_blocks(proj, read, first, chunks):
+    def read_blocks(proj, read, first, chunks, middle=None):
         def scores_of(i):
             rows = slice(i * BLOCK, (i + 1) * BLOCK)
             return [
@@ -388,6 +390,8 @@
             if i + 1 < half_blocks:
                 raw = scores_of(i + 1)
             read_out(i, *parts)
+            if middle is not None and i + 1 == half_blocks // 2:
+                middle()
         for chunk in chunks[half_blocks:]:
             chunk()
 
@@ -446,8 +450,10 @@
 
     along_x, along_z = lax.rem(me, 4), me // 4
     lateness = 2 * along_z + jnp.where(along_x == 3, 3, 2 * along_x)
-    late = lateness >= 6
-    early = lateness < 4
+    late = lateness >= 7
+    between = (lateness >= 4) & (lateness < 7)
+    soon = (lateness >= 1) & (lateness < 4)
+    first = lateness < 1
     pl.when(late)(owner_step)
 
     prod_piece(x_peer, proj_peer, peer_row, 0)
@@ -465,38 +471,29 @@
     def _():
         rim_copy(me + 1).start()
 
-    pl.when(jnp.logical_not(late | early))(owner_step)
+    pl.when(between)(owner_step)
 
     read_blocks(
         proj_peer, read_peer, peer_block,
         [
+            lambda: piece_of(GO_, x_peer, proj_peer, 0),
+            lambda: piece_of(GO_, x_peer, proj_peer, 1),
             lambda: piece_of(GO_, x_own, proj_own, 0),
             lambda: piece_of(GO_, x_own, proj_own, 1),
-            lambda: piece_of(GO_, x_peer, proj_peer, 0),
-            lambda: piece_of(GO_, x_peer, proj_peer, 1),
         ],
+        middle=lambda: pl.when(soon)(owner_step),
     )
 
-    pl.when(early)(owner_step)
+    pl.when(first)(owner_step)
 
     taps_copy.wait()
     for copy in out_copies:
         copy.wait()
-
-    @pl.when(me == 0)
-    def _():
-        rim_in[...] = jnp.zeros_like(rim_in)
-
-    @pl.when(me > 0)
-    def _():
-        rim_copy(me - 1).wait_recv()
-
-    prod[0:16, :] = rim_in[...]
     tap_rows = taps[:, pl.ds(my_lane, local_width)].astype(F32)
     conv_rows = 64
 
-    def convolve(proj, dst, first):
-        for i in range(own // conv_rows):
+    def convolve(proj, dst, first, part):
+        for i in part:
             row = pl.multiple_of(first + i * conv_rows, conv_rows)
             rows = slice(i * conv_rows, (i + 1) * conv_rows)
             window = prod[pl.ds(row, conv_rows + 16), :].astype(F32)
@@ -505,13 +502,20 @@
             mixed = mixed + window[16 : 16 + conv_rows] * tap_rows[2:3]
             dst[rows, :] = (proj[GO_][rows, :].astype(F32) * mixed).astype(BF16)
 
-    convolve(proj_peer, conv_peer, peer_row)
-    send_conv = pltpu.make_async_remote_copy(
-        src_ref=conv_peer, dst_ref=conv_in, send_sem=conv_s, recv_sem=conv_r, **peer
-    )
-    project_sig(x_peer, sig_peer)
-    send_conv.start()
-    convolve(proj_own, conv_own, my_row)
+    conv_steps = range(own // conv_rows)
+
+    def send_conv(i):
+        at = (pl.ds(conv_rows, own - conv_rows), pl.ds(0, conv_rows))[i]
+        return pltpu.make_async_remote_copy(
+            src_ref=conv_peer.at[at, :], dst_ref=conv_in.at[at, :],
+            send_sem=conv_s.at[i], recv_sem=conv_r.at[i], **peer,
+        )
+
+    sig_piece(x_peer, sig_peer, 0)
+    convolve(proj_peer, conv_peer, peer_row, conv_steps[1:])
+    send_conv(0).start()
+    sig_piece(x_peer, sig_peer, 1)
+    convolve(proj_own, conv_own, my_row, conv_steps[1:])
     start_log = jnp.zeros((heads, BLOCK), F32)
     for i in range(n_sp - 1):
         merged = jnp.maximum(scal_in[i, 0:heads, :] + start_log, scal_in[i, heads : 2 * heads, :])
@@ -523,7 +527,39 @@
     for b in range(nblocks):
         rows = slice(b * heads, (b + 1) * heads)
         cols_in[b] = jnp.concatenate([keep[rows], bring[rows], fill], axis=0).T
-    acc[...] = jnp.dot(conv_own[...], woc[...], preferred_element_type=F32)
+
+    @pl.when(me == 0)
+    def _():
+        rim_in[...] = jnp.zeros_like(rim_in)
+
+    @pl.when(me > 0)
+    def _():
+        rim_copy(me - 1).wait_recv()
+
+    prod[0:16, :] = rim_in[...]
+    convolve(proj_peer, conv_peer, peer_row, conv_steps[:1])
+    convolve(proj_own, conv_own, my_row, conv_steps[:1])
+    send_conv(1).start()
+
+    def scale_parts(proj, read, first):
+        for block in range(half_blocks):
+            rows = slice(block * BLOCK, (block + 1) * BLOCK)
+            columns = cols_in[first + block]
+            for h in range(heads):
+                hs = slice(h * dh, (h + 1) * dh)
+                read[rows, hs] = columns[:, h : h + 1] * read[rows, hs]
+                proj[Q_][rows, hs] = (
+                    columns[:, heads + h : heads + h + 1] * proj[Q_][rows, hs].astype(F32)
+                ).astype(BF16)
+
+    column = acc.shape[1] // 4
+    for j in range(4):
+        at = slice(j * column, (j + 1) * column)
+        acc[:, at] = jnp.dot(conv_own[...], woc[:, at], preferred_element_type=F32)
+        if j == 0:
+            scale_parts(proj_peer, read_peer, peer_block)
+        if j == 2:
+            scale_parts(proj_own, read_own, my_block)
 
     def wait_state(k, carry):
         source = lax.rem(me + k, n_sp)
@@ -534,7 +570,8 @@
         return carry
 
     lax.fori_loop(1, n_sp, wait_state, 0)
-    send_conv.wait_recv()
+    for i in range(2):
+        send_conv(i).wait_recv()
     for copy in out_weights:
         copy.wait_recv()
 
@@ -553,17 +590,13 @@
             for block in range(piece * piece_blocks, (piece + 1) * piece_blocks)
         ]
 
-    def finish(brought, read, sig, dst, piece, first):
+    def finish(brought, read, sig, dst, piece):
         for i in range(piece_blocks):
             block = piece * piece_blocks + i
             rows = slice(block * BLOCK, (block + 1) * BLOCK)
-            columns = cols_in[first + block]
             for h in range(heads):
                 hs = slice(h * dh, (h + 1) * dh)
-                readout = (
-                    columns[:, h : h + 1] * read[rows, hs]
-                    + columns[:, heads + h : heads + h + 1] * brought[i][h]
-                )
+                readout = read[rows, hs] + brought[i][h]
                 normalized = readout * lax.rsqrt(
                     jnp.mean(readout * readout, axis=-1, keepdims=True) + EPSILON
                 )
@@ -574,30 +607,36 @@
             src_ref=mem, dst_ref=mem_in.at[i], send_sem=mem_s.at[i], recv_sem=mem_r.at[i], **peer
         )
 
-    def add_part(at, rows, weight):
-        acc[at, :] = acc[at, :] + jnp.dot(rows, weight[...], preferred_element_type=F32)
+    def conv_part(j):
+        at = slice(j * column, (j + 1) * column)
+        acc[:, at] = acc[:, at] + jnp.dot(
+            conv_in[...], woc_in[:, at], preferred_element_type=F32
+        )
+
+    def own_part(i, mem):
+        acc[spans[i], :] = acc[spans[i], :] + jnp.dot(
+            mem[...], wom[...], preferred_element_type=F32
+        )
 
     brought_0 = bring_in(proj_peer, 0)
+    conv_part(0)
     brought_1 = bring_in(proj_peer, 1)
-    finish(brought_0, read_peer, sig_peer, mem_0, 0, peer_block)
+    finish(brought_0, read_peer, sig_peer, mem_0, 0)
     send_memory(0, mem_0).start()
-    add_part(spans[0], conv_in[spans[0], :], woc_in)
-    finish(brought_1, read_peer, sig_peer, mem_1, 1, peer_block)
+    conv_part(1)
+    brought_2 = bring_in(proj_own, 0)
+    finish(brought_1, read_peer, sig_peer, mem_1, 1)
     send_memory(1, mem_1).start()
-    brought_2 = bring_in(proj_own, 0)
-    finish(brought_2, read_own, sig_own, mem_2, 0, my_block)
-    add_part(spans[1], conv_in[spans[1], :], woc_in)
+    conv_part(2)
     brought_3 = bring_in(proj_own, 1)
-    finish(brought_3, read_own, sig_own, mem_3, 1, my_block)
-    add_part(spans[0], mem_2[...], wom)
-    add_part(spans[1], mem_3[...], wom)
-
-    for i, at in enumerate(spans):
+    finish(brought_2, read_own, sig_own, mem_2, 0)
+    conv_part(3)
+    finish(brought_3, read_own, sig_own, mem_3, 1)
+    own_part(0, mem_2)
+    own_part(1, mem_3)
+
+    for i in range(pieces):
         send_memory(i, (mem_0, mem_1)[i]).wait_recv()
-    for i, at in enumerate(spans):
-        out[0, at, :] = (
-            acc[at, :] + jnp.dot(mem_in[i], wom_in[...], preferred_element_type=F32)
-        ).astype(BF16)
 
     send_rows.wait_send()
     send_gates.wait_send()
@@ -617,23 +656,31 @@
         return carry
 
     lax.fori_loop(1, n_sp, drain, 0)
-    send_conv.wait_send()
+    for i in range(2):
+        send_conv(i).wait_send()
     for copy in out_weights:
         copy.wait_send()
     for i, mem in enumerate((mem_0, mem_1)):
         send_memory(i, mem).wait_send()
 
 
-def store_kernel(src, dst, sems):
-    rows = src.shape[1] // 4
-    copies = [
-        pltpu.make_async_copy(
-            src.at[0, pl.ds(i * rows, rows), :], dst.at[0, pl.ds(i * rows, rows), :], sems.at[i]
-        )
-        for i in range(4)
-    ]
-    for copy in copies:
+def last_kernel(acc, mem_in, wom_in, out, stage, sems):
+    rows = acc.shape[0] // 4
+    copies = []
+    for i in range(4):
+        at = slice(i * rows, (i + 1) * rows)
+        stage[at, :] = (
+            acc[at, :]
+            + jnp.dot(
+                mem_in[i // 2, (i % 2) * rows : (i % 2 + 1) * rows, :], wom_in[...],
+                preferred_element_type=F32,
+            )
+        ).astype(BF16)
+        copy = pltpu.make_async_copy(
+            stage.at[pl.ds(i * rows, rows), :], out.at[0, pl.ds(i * rows, rows), :], sems.at[i]
+        )
         copy.start()
+        copies.append(copy)
     for copy in copies:
         copy.wait()
 
@@ -677,10 +724,7 @@
         half_wide, half_wide,
         half_wide, half_wide,
         half, half, half,
-        vmem((own, width), F32),
         quarter, quarter, quarter, quarter,
-        vmem((2, own // 2, local_width), BF16),
-        vmem((local_width, width), BF16),
         vmem((local_width, width), BF16),
         vmem((nblocks, heads, dh, 2 * BLOCK), BF16),
         vmem((6, nblocks * heads, BLOCK), F32),
@@ -703,17 +747,21 @@
         dma((n_sp,)), dma((n_sp,)),
         dma, dma,
         dma((2,)), dma((2,)),
-        dma, dma,
+        dma((2,)), dma((2,)),
         dma((2,)), dma((2,)),
     ]
-    rows = pl.pallas_call(
+    acc, mem_in, wom_in = pl.pallas_call(
         functools.partial(kernel, n_sp),
-        out_shape=vmem(tokens.shape, BF16),
+        out_shape=(
+            vmem((own, width), F32),
+            vmem((2, own // 2, local_width), BF16),
+            vmem((local_width, width), BF16),
+        ),
         in_specs=[pl.BlockSpec(memory_space=pl.ANY)] * 19,
-        out_specs=pl.BlockSpec(memory_space=pltpu.VMEM),
+        out_specs=(pl.BlockSpec(memory_space=pltpu.VMEM),) * 3,
         scratch_shapes=scratch,
         compiler_params=pltpu.CompilerParams(
-            collective_id=0, has_side_effects=True, vmem_limit_bytes=58 * 1024 * 1024
+            collective_id=0, has_side_effects=True, vmem_limit_bytes=54 * 1024 * 1024
         ),
     )(
         tokens, norm_gain.reshape(-1, 128),
@@ -723,12 +771,13 @@
         out_memory, out_conv,
     )
     return pl.pallas_call(
-        store_kernel,
+        last_kernel,
         out_shape=jax.ShapeDtypeStruct(tokens.shape, BF16),
-        in_specs=[pl.BlockSpec(memory_space=pltpu.VMEM)],
+        in_specs=[pl.BlockSpec(memory_space=pltpu.VMEM)] * 3,
         out_specs=pl.BlockSpec(memory_space=pl.ANY),
-        scratch_shapes=[dma((4,))],
-    )(pltpu.with_memory_space_constraint(rows, pltpu.VMEM))
+        scratch_shapes=[vmem((own, width), BF16), dma((4,))],
+        compiler_params=pltpu.CompilerParams(vmem_limit_bytes=16 * 1024 * 1024),
+    )(*(pltpu.with_memory_space_constraint(part, pltpu.VMEM) for part in (acc, mem_in, wom_in)))
 
 
 def solution(mesh):

time: 34.8 us -> 32.2 us (0.925); the launches traced: 34.2 us -> 32.1 us
  Pallas kernels: 34.1 us -> 31.9 us
    pallas_call x2, Pallas kernels: 34.1 us -> 31.9 us  [the longest x1 29.8 us: local_layer(): pl.pallas_call(functools.partial(kernel, n_sp), out_shape=(vmem((own, wid...]
where the time goes in v4:
time: 32.2 us; the launch traced here: 32.1 us
  Pallas kernels  31.9 us (99%)
    pallas_call x1, Pallas kernels, local_layer(): pl.pallas_call(functools.partial(kernel, n_sp), out_shape=(vmem((own, wid...  29.8 us
    pallas_call x1, Pallas kernels, local_layer(): pl.pallas_call(last_kernel, out_shape=jax.ShapeDtypeStruct(tokens.shape,...  2.1 us

profile of v4, /device:TPU:1, one launch (start us, length us, event | category | flops | bytes accessed | tf_op | source)
XLA Modules:
  0.0 32.1 jit_solution(7758994593565926261)
XLA Ops:
  0.0 29.8 %shard_map.181 = (f32[512,2048]{1,0:T(8,128)S(1)}, bf16[2,256,512]{2,1,0:T(8,128)(2,1)S(1)}, bf16[512,2048]{1,0:T(8,128)(2,1)S(1)}) custom-call(bf16[1,512,2048]{2,1,0:T(8,128)(2,1)} %tokens.1, bf16[16,128]{1,0:T(8,128)(2,1)} %bitcast.10, bf16[2048,512]{1,0:T(8,128)(2,1)} %w_query.1, bf16[2048,512]{1,0:T(8,128)(2,1)} %w_key.1, bf16[2048,512]{1,0:T(8,128)(2,1)} %w_value.1, ...), custom_call_target="tpu_custom_call" | custom-call | tf_op jit(solution)/shard_map/pallas_call | solution.py:753
  29.8 2.1 %shard_map.182 = bf16[1,512,2048]{2,1,0:T(8,128)(2,1)} custom-call(f32[512,2048]{1,0:T(8,128)S(1)} %get-tuple-element.8.acc, bf16[2,256,512]{2,1,0:T(8,128)(2,1)S(1)} %get-tuple-element.9.mem_in, bf16[512,2048]{1,0:T(8,128)(2,1)S(1)} %get-tuple-element.10.wom_in), custom_call_target="tpu_custom_call" | custom-call | tf_op jit(solution)/shard_map/pallas_call | solution.py:773

commit v5 on v4

--- a/solution.py
+++ b/solution.py
@@ -32,7 +32,7 @@
     x_own, x_peer, proj_own, proj_peer, sig_own, sig_peer, read_own, read_peer,
     conv_own, conv_peer, conv_in, mem_0, mem_1, mem_2, mem_3, woc_in,
     keys, table, cols, cols_in, terms, seg, seg_in, scal, scal_in, state_out, state_in,
-    rim_in, prod,
+    rim_in, rim_out, prod_own, prod_peer,
     ready, lsem, tok_s, tok_r, gate_s, gate_r, seg_s, seg_r, scal_s, scal_r, st_s, st_r,
     rim_s, rim_r, ow_s, ow_r, conv_s, conv_r, mem_s, mem_r,
 ):
@@ -106,7 +106,7 @@
     gain_row = jnp.concatenate(
         [gain[i : i + 1, :] for i in range(gain.shape[0])], axis=1
     ).astype(F32)
-    norm_rows = 16
+    norm_rows = 8
 
     def own_gates(c):
         rows = x_own[c * chunk_rows : (c + 1) * chunk_rows, :]
@@ -176,12 +176,16 @@
             rows[at, :], w_all[p][...], preferred_element_type=F32
         ).astype(BF16)
 
-    def prod_piece(rows, proj, row, i):
+    lane_tiles = range(local_width // 128)
+
+    def prod_piece(rows, proj, prod, i):
         at = spans[i]
         value = jnp.dot(rows[at, :], w_all[CI_][...], preferred_element_type=F32).astype(BF16)
-        prod[pl.ds(row + 16 + i * piece_rows, piece_rows), :] = (
-            proj[GI_][at, :].astype(F32) * value.astype(F32)
-        ).astype(BF16)
+        product = (proj[GI_][at, :].astype(F32) * value.astype(F32)).astype(BF16).astype(F32)
+        for c in lane_tiles:
+            prod[c, 8 + i * piece_rows : 8 + (i + 1) * piece_rows, :] = product[
+                :, c * 128 : (c + 1) * 128
+            ]
 
     w_copies[K_].wait()
     w_copies[V_].wait()
@@ -334,13 +338,24 @@
         return (
             pltpu.make_async_remote_copy(
                 src_ref=scal, dst_ref=scal_in.at[me],
-                send_sem=scal_s.at[target], recv_sem=scal_r.at[me], **sp(target),
+                send_sem=scal_s, recv_sem=scal_r, **sp(target),
             ),
             pltpu.make_async_remote_copy(
                 src_ref=seg.at[target], dst_ref=seg_in.at[me],
-                send_sem=seg_s.at[target], recv_sem=seg_r.at[me], **sp(target),
+                send_sem=seg_s, recv_sem=seg_r, **sp(target),
             ),
         )
+
+    def all_copies(dst, send, recv):
+        slots = dst.at[pl.ds(0, n_sp - 1)]
+        return pltpu.make_async_remote_copy(
+            src_ref=slots, dst_ref=slots, send_sem=send, recv_sem=recv,
+            **sp(lax.rem(me + 1, n_sp)),
+        )
+
+    all_scales = all_copies(scal_in, scal_s, scal_r)
+    all_segments = all_copies(seg_in, seg_s, seg_r)
+    all_states = all_copies(state_in, st_s, st_r)
 
     for k in range(1, n_sp):
         for copy in segment_copies(lax.rem(me + k, n_sp)):
@@ -398,30 +413,33 @@
     read_blocks(
         proj_own, read_own, my_block,
         [
-            lambda: prod_piece(x_own, proj_own, my_row, 0),
-            lambda: prod_piece(x_own, proj_own, my_row, 1),
+            lambda: prod_piece(x_own, proj_own, prod_own, 0),
+            lambda: prod_piece(x_own, proj_own, prod_own, 1),
             lambda: piece_of(GI_, x_peer, proj_peer, 0),
             lambda: piece_of(GI_, x_peer, proj_peer, 1),
         ],
     )
-    project(Q_, x_peer, proj_peer)
+    prod_piece(x_peer, proj_peer, prod_peer, 0)
+    prod_piece(x_peer, proj_peer, prod_peer, 1)
+
+    def rim_copy(target):
+        return pltpu.make_async_remote_copy(
+            src_ref=rim_out, dst_ref=rim_in,
+            send_sem=rim_s, recv_sem=rim_r, **sp(target),
+        )
+
+    last = me == n_sp - 1
+    rim_out[...] = jnp.where(side == 0, prod_peer[:, own : own + 8, :], prod_own[:, own : own + 8, :])
+
+    @pl.when(jnp.logical_not(last))
+    def _():
+        rim_copy(me + 1).start()
 
     def owner_step():
         init_copy.wait()
 
-        def wait_segment(k, carry):
-            source = lax.rem(me + k, n_sp)
-            pltpu.make_async_remote_copy(
-                src_ref=scal, dst_ref=scal_in.at[source],
-                send_sem=scal_s.at[source], recv_sem=scal_r.at[source], **sp(source),
-            ).wait_recv()
-            pltpu.make_async_remote_copy(
-                src_ref=seg.at[source], dst_ref=seg_in.at[source],
-                send_sem=seg_s.at[source], recv_sem=seg_r.at[source], **sp(source),
-            ).wait_recv()
-            return carry
-
-        lax.fori_loop(1, n_sp, wait_segment, 0)
+        all_scales.wait_recv()
+        all_segments.wait_recv()
         state = init[...]
         state_log = jnp.zeros((1, BLOCK), F32)
         for i in range(n_sp):
@@ -438,15 +456,12 @@
             state_log = merged
         state_in[me] = state_out[me]
 
-        def send_state(k, carry):
+        for k in range(1, n_sp):
             target = lax.rem(me + k, n_sp)
             pltpu.make_async_remote_copy(
                 src_ref=state_out.at[target], dst_ref=state_in.at[me],
-                send_sem=st_s.at[target], recv_sem=st_r.at[me], **sp(target),
+                send_sem=st_s, recv_sem=st_r, **sp(target),
             ).start()
-            return carry
-
-        lax.fori_loop(1, n_sp, send_state, 0)
 
     along_x, along_z = lax.rem(me, 4), me // 4
     lateness = 2 * along_z + jnp.where(along_x == 3, 3, 2 * along_x)
@@ -456,20 +471,7 @@
     first = lateness < 1
     pl.when(late)(owner_step)
 
-    prod_piece(x_peer, proj_peer, peer_row, 0)
-    prod_piece(x_peer, proj_peer, peer_row, 1)
-
-    def rim_copy(target):
-        return pltpu.make_async_remote_copy(
-            src_ref=prod.at[pl.ds(count, 16), :], dst_ref=rim_in,
-            send_sem=rim_s, recv_sem=rim_r, **sp(target),
-        )
-
-    last = me == n_sp - 1
-
-    @pl.when(jnp.logical_not(last))
-    def _():
-        rim_copy(me + 1).start()
+    project(Q_, x_peer, proj_peer)
 
     pl.when(between)(owner_step)
 
@@ -492,30 +494,36 @@
     tap_rows = taps[:, pl.ds(my_lane, local_width)].astype(F32)
     conv_rows = 64
 
-    def convolve(proj, dst, first, part):
+    def convolve(proj, prod, dst, part):
         for i in part:
-            row = pl.multiple_of(first + i * conv_rows, conv_rows)
             rows = slice(i * conv_rows, (i + 1) * conv_rows)
-            window = prod[pl.ds(row, conv_rows + 16), :].astype(F32)
-            mixed = window[14 : 14 + conv_rows] * tap_rows[0:1]
-            mixed = mixed + window[15 : 15 + conv_rows] * tap_rows[1:2]
-            mixed = mixed + window[16 : 16 + conv_rows] * tap_rows[2:3]
-            dst[rows, :] = (proj[GO_][rows, :].astype(F32) * mixed).astype(BF16)
+            for c in lane_tiles:
+                lanes_at = slice(c * 128, (c + 1) * 128)
+                mixed = prod[c, i * conv_rows + 6 : i * conv_rows + 6 + conv_rows, :] * tap_rows[
+                    0:1, lanes_at
+                ]
+                for j in range(1, 3):
+                    start = i * conv_rows + 6 + j
+                    mixed = mixed + prod[c, start : start + conv_rows, :] * tap_rows[
+                        j : j + 1, lanes_at
+                    ]
+                dst[rows, lanes_at] = (proj[GO_][rows, lanes_at].astype(F32) * mixed).astype(BF16)
 
     conv_steps = range(own // conv_rows)
-
-    def send_conv(i):
-        at = (pl.ds(conv_rows, own - conv_rows), pl.ds(0, conv_rows))[i]
-        return pltpu.make_async_remote_copy(
-            src_ref=conv_peer.at[at, :], dst_ref=conv_in.at[at, :],
-            send_sem=conv_s.at[i], recv_sem=conv_r.at[i], **peer,
-        )
-
-    sig_piece(x_peer, sig_peer, 0)
-    convolve(proj_peer, conv_peer, peer_row, conv_steps[1:])
-    send_conv(0).start()
-    sig_piece(x_peer, sig_peer, 1)
-    convolve(proj_own, conv_own, my_row, conv_steps[1:])
+    send_conv = pltpu.make_async_remote_copy(
+        src_ref=conv_peer, dst_ref=conv_in, send_sem=conv_s, recv_sem=conv_r, **peer
+    )
+
+    @pl.when(me == 0)
+    def _():
+        rim_in[...] = jnp.zeros_like(rim_in)
+
+    @pl.when(me > 0)
+    def _():
+        rim_copy(me - 1).wait_recv()
+
+    prod_own[:, 0:8, :] = jnp.where(side == 0, rim_in[...], prod_peer[:, own : own + 8, :])
+    prod_peer[:, 0:8, :] = jnp.where(side == 0, prod_own[:, own : own + 8, :], rim_in[...])
     start_log = jnp.zeros((heads, BLOCK), F32)
     for i in range(n_sp - 1):
         merged = jnp.maximum(scal_in[i, 0:heads, :] + start_log, scal_in[i, heads : 2 * heads, :])
@@ -528,19 +536,6 @@
         rows = slice(b * heads, (b + 1) * heads)
         cols_in[b] = jnp.concatenate([keep[rows], bring[rows], fill], axis=0).T
 
-    @pl.when(me == 0)
-    def _():
-        rim_in[...] = jnp.zeros_like(rim_in)
-
-    @pl.when(me > 0)
-    def _():
-        rim_copy(me - 1).wait_recv()
-
-    prod[0:16, :] = rim_in[...]
-    convolve(proj_peer, conv_peer, peer_row, conv_steps[:1])
-    convolve(proj_own, conv_own, my_row, conv_steps[:1])
-    send_conv(1).start()
-
     def scale_parts(proj, read, first):
         for block in range(half_blocks):
             rows = slice(block * BLOCK, (block + 1) * BLOCK)
@@ -552,26 +547,22 @@
                     columns[:, heads + h : heads + h + 1] * proj[Q_][rows, hs].astype(F32)
                 ).astype(BF16)
 
+    half_steps = len(conv_steps) // 2
+    convolve(proj_peer, prod_peer, conv_peer, conv_steps[:half_steps])
+    sig_piece(x_peer, sig_peer, 0)
+    convolve(proj_peer, prod_peer, conv_peer, conv_steps[half_steps:])
+    send_conv.start()
+    scale_parts(proj_peer, read_peer, peer_block)
+    sig_piece(x_peer, sig_peer, 1)
+    convolve(proj_own, prod_own, conv_own, conv_steps[:half_steps])
+    acc[spans[0], :] = jnp.dot(conv_own[spans[0], :], woc[...], preferred_element_type=F32)
+    convolve(proj_own, prod_own, conv_own, conv_steps[half_steps:])
+    scale_parts(proj_own, read_own, my_block)
+    acc[spans[1], :] = jnp.dot(conv_own[spans[1], :], woc[...], preferred_element_type=F32)
     column = acc.shape[1] // 4
-    for j in range(4):
-        at = slice(j * column, (j + 1) * column)
-        acc[:, at] = jnp.dot(conv_own[...], woc[:, at], preferred_element_type=F32)
-        if j == 0:
-            scale_parts(proj_peer, read_peer, peer_block)
-        if j == 2:
-            scale_parts(proj_own, read_own, my_block)
-
-    def wait_state(k, carry):
-        source = lax.rem(me + k, n_sp)
-        pltpu.make_async_remote_copy(
-            src_ref=state_out.at[source], dst_ref=state_in.at[source],
-            send_sem=st_s.at[source], recv_sem=st_r.at[source], **sp(source),
-        ).wait_recv()
-        return carry
-
-    lax.fori_loop(1, n_sp, wait_state, 0)
-    for i in range(2):
-        send_conv(i).wait_recv()
+
+    all_states.wait_recv()
+    send_conv.wait_recv()
     for copy in out_weights:
         copy.wait_recv()
 
@@ -645,19 +636,10 @@
     def _():
         rim_copy(me + 1).wait_send()
 
-    def drain(k, carry):
-        target = lax.rem(me + k, n_sp)
-        for copy in segment_copies(target):
-            copy.wait_send()
-        pltpu.make_async_remote_copy(
-            src_ref=state_out.at[target], dst_ref=state_in.at[me],
-            send_sem=st_s.at[target], recv_sem=st_r.at[me], **sp(target),
-        ).wait_send()
-        return carry
-
-    lax.fori_loop(1, n_sp, drain, 0)
-    for i in range(2):
-        send_conv(i).wait_send()
+    all_scales.wait_send()
+    all_segments.wait_send()
+    all_states.wait_send()
+    send_conv.wait_send()
     for copy in out_weights:
         copy.wait_send()
     for i, mem in enumerate((mem_0, mem_1)):
@@ -737,17 +719,17 @@
         vmem((n_sp, 2 * heads, BLOCK), F32),
         vmem((n_sp, slice_rows, dh), BF16),
         vmem((n_sp, slice_rows, dh), BF16),
-        vmem((16, local_width), BF16),
-        vmem((count + 16, local_width), BF16),
+        vmem((local_width // 128, 8, 128), F32),
+        vmem((local_width // 128, 8, 128), F32),
+        vmem((local_width // 128, own + 8, 128), F32),
+        vmem((local_width // 128, own + 8, 128), F32),
         pltpu.SemaphoreType.REGULAR,
         dma((L_W + 7,)),
         dma, dma, dma, dma,
-        dma((n_sp,)), dma((n_sp,)),
-        dma((n_sp,)), dma((n_sp,)),
-        dma((n_sp,)), dma((n_sp,)),
+        dma, dma, dma, dma, dma, dma,
         dma, dma,
         dma((2,)), dma((2,)),
-        dma((2,)), dma((2,)),
+        dma, dma,
         dma((2,)), dma((2,)),
     ]
     acc, mem_in, wom_in = pl.pallas_call(

time: 32.2 us -> 30.7 us (0.953)
  Pallas kernels: 31.9 us -> 30.5 us
    pallas_call x1, Pallas kernels: 29.8 us -> 28.4 us  [local_layer(): pl.pallas_call(functools.partial(kernel, n_sp), out_shape=(vmem((own, wid...]
where the time goes in v5:
time: 30.7 us; the launch traced here: 30.6 us
  Pallas kernels  30.5 us (99%)
    pallas_call x1, Pallas kernels, local_layer(): pl.pallas_call(functools.partial(kernel, n_sp), out_shape=(vmem((own, wid...  28.4 us
    pallas_call x1, Pallas kernels, local_layer(): pl.pallas_call(last_kernel, out_shape=jax.ShapeDtypeStruct(tokens.shape,...  2.11 us

profile of v5, /device:TPU:1, one launch (start us, length us, event | category | flops | bytes accessed | tf_op | source)
XLA Modules:
  0.0 30.6 jit_solution(7739501374365723473)
XLA Ops:
  0.0 28.4 %shard_map.181 = (f32[512,2048]{1,0:T(8,128)S(1)}, bf16[2,256,512]{2,1,0:T(8,128)(2,1)S(1)}, bf16[512,2048]{1,0:T(8,128)(2,1)S(1)}) custom-call(bf16[1,512,2048]{2,1,0:T(8,128)(2,1)} %tokens.1, bf16[16,128]{1,0:T(8,128)(2,1)} %bitcast.10, bf16[2048,512]{1,0:T(8,128)(2,1)} %w_query.1, bf16[2048,512]{1,0:T(8,128)(2,1)} %w_key.1, bf16[2048,512]{1,0:T(8,128)(2,1)} %w_value.1, ...), custom_call_target="tpu_custom_call" | custom-call | tf_op jit(solution)/shard_map/pallas_call | solution.py:735
  28.4 2.1 %shard_map.182 = bf16[1,512,2048]{2,1,0:T(8,128)(2,1)} custom-call(f32[512,2048]{1,0:T(8,128)S(1)} %get-tuple-element.8.acc, bf16[2,256,512]{2,1,0:T(8,128)(2,1)S(1)} %get-tuple-element.9.mem_in, bf16[512,2048]{1,0:T(8,128)(2,1)S(1)} %get-tuple-element.10.wom_in), custom_call_target="tpu_custom_call" | custom-call | tf_op jit(solution)/shard_map/pallas_call | solution.py:755

commit v6 on v5

--- a/solution.py
+++ b/solution.py
@@ -28,7 +28,7 @@
     w_igate, w_fgate, input_bias, forget_bias, forget_extra, init_memory, head_gain, conv_taps,
     out_memory, out_conv,
     acc, mem_in, wom_in,
-    tok, gain, w_all, wom, woc, wig, wfg, gates, fe, ib, fb, taps, hg, init,
+    tok, gain, w_all, wom, woc, wig, wfg, gates, fe, ib, fb, taps, hg, init, entry,
     x_own, x_peer, proj_own, proj_peer, sig_own, sig_peer, read_own, read_peer,
     conv_own, conv_peer, conv_in, mem_0, mem_1, mem_2, mem_3, woc_in,
     keys, table, cols, cols_in, terms, seg, seg_in, scal, scal_in, state_out, state_in,
@@ -89,7 +89,7 @@
     ]
     head_copy = local(head_gain, hg, L_HG)
     taps_copy = local(conv_taps, taps, L_TAPS)
-    init_copy = local(init_memory.at[0, my_head, pl.ds(my_depth, slice_rows), :], init, L_INIT)
+    init_copy = local(init_memory.at[0], init, L_INIT)
     out_copies = [local(out_conv, woc, L_OC), local(out_memory, wom, L_OM)]
     gain_copy.start()
     for copy in token_copies + narrow_copies + w_copies[:2] + gate_copies:
@@ -108,9 +108,11 @@
     ).astype(F32)
     norm_rows = 8
 
+    gate_rows = chunk_rows
+
     def own_gates(c):
-        rows = x_own[c * chunk_rows : (c + 1) * chunk_rows, :]
-        gates[:, pl.ds(my_row + c * chunk_rows, chunk_rows)] = lax.dot_general(
+        rows = x_own[c * gate_rows : (c + 1) * gate_rows, :]
+        gates[:, pl.ds(my_row + c * gate_rows, gate_rows)] = lax.dot_general(
             narrow, rows, (((1,), (1,)), ((), ())), preferred_element_type=F32
         )
 
@@ -321,6 +323,19 @@
     def _():
         pl.semaphore_wait(ready, n_sp - 1 - me)
 
+    along_x, along_z, size_z = lax.rem(me, 4), me // 4, n_sp // 4
+    steps = sorted(
+        ((dx, dz) for dx in range(4) for dz in range(size_z) if dx or dz),
+        key=lambda step: -min(step[0], 4 - step[0]) - min(step[1], size_z - step[1]),
+    )
+    targets = [
+        lax.rem(along_z + dz, size_z) * 4 + lax.rem(along_x + dx, 4) for dx, dz in steps
+    ]
+    for target in targets:
+        pltpu.make_async_remote_copy(
+            src_ref=scal, dst_ref=scal_in.at[me],
+            send_sem=scal_s, recv_sem=scal_r, **sp(target),
+        ).start()
     piece_of(GI_, x_own, proj_own, 0)
     for h in range(heads):
         held = jnp.zeros((dh, dh), F32)
@@ -334,18 +349,6 @@
             ].astype(BF16)
     seg_in[me] = seg[me]
 
-    def segment_copies(target):
-        return (
-            pltpu.make_async_remote_copy(
-                src_ref=scal, dst_ref=scal_in.at[me],
-                send_sem=scal_s, recv_sem=scal_r, **sp(target),
-            ),
-            pltpu.make_async_remote_copy(
-                src_ref=seg.at[target], dst_ref=seg_in.at[me],
-                send_sem=seg_s, recv_sem=seg_r, **sp(target),
-            ),
-        )
-
     def all_copies(dst, send, recv):
         slots = dst.at[pl.ds(0, n_sp - 1)]
         return pltpu.make_async_remote_copy(
@@ -357,9 +360,11 @@
     all_segments = all_copies(seg_in, seg_s, seg_r)
     all_states = all_copies(state_in, st_s, st_r)
 
-    for k in range(1, n_sp):
-        for copy in segment_copies(lax.rem(me + k, n_sp)):
-            copy.start()
+    for target in targets:
+        pltpu.make_async_remote_copy(
+            src_ref=seg.at[target], dst_ref=seg_in.at[me],
+            send_sem=seg_s, recv_sem=seg_r, **sp(target),
+        ).start()
     piece_of(GI_, x_own, proj_own, 1)
 
     t_index = lax.broadcasted_iota(jnp.int32, (BLOCK, BLOCK), 0)
@@ -440,7 +445,7 @@
 
         all_scales.wait_recv()
         all_segments.wait_recv()
-        state = init[...]
+        state = init[my_head, pl.ds(my_depth, slice_rows), :]
         state_log = jnp.zeros((1, BLOCK), F32)
         for i in range(n_sp):
             state_out[i] = state.astype(BF16)
@@ -456,15 +461,13 @@
             state_log = merged
         state_in[me] = state_out[me]
 
-        for k in range(1, n_sp):
-            target = lax.rem(me + k, n_sp)
+        for target in targets:
             pltpu.make_async_remote_copy(
                 src_ref=state_out.at[target], dst_ref=state_in.at[me],
                 send_sem=st_s, recv_sem=st_r, **sp(target),
             ).start()
 
-    along_x, along_z = lax.rem(me, 4), me // 4
-    lateness = 2 * along_z + jnp.where(along_x == 3, 3, 2 * along_x)
+    lateness = 2 * along_z + jnp.where(along_x == 1, 2, jnp.where(along_x == 0, 0, 3))
     late = lateness >= 7
     between = (lateness >= 4) & (lateness < 7)
     soon = (lateness >= 1) & (lateness < 4)
@@ -561,7 +564,15 @@
     acc[spans[1], :] = jnp.dot(conv_own[spans[1], :], woc[...], preferred_element_type=F32)
     column = acc.shape[1] // 4
 
-    all_states.wait_recv()
+    @pl.when(me == 0)
+    def _():
+        entry[...] = init[...].reshape(entry.shape).astype(BF16)
+
+    @pl.when(me > 0)
+    def _():
+        all_states.wait_recv()
+        entry[...] = state_in[...]
+
     send_conv.wait_recv()
     for copy in out_weights:
         copy.wait_recv()
@@ -573,7 +584,7 @@
             [
                 jnp.dot(
                     proj[Q_][block * BLOCK : (block + 1) * BLOCK, h * dh : (h + 1) * dh],
-                    state_in[h * per_head : (h + 1) * per_head].reshape(dh, dh),
+                    entry[h * per_head : (h + 1) * per_head].reshape(dh, dh),
                     preferred_element_type=F32,
                 )
                 for h in range(heads)
@@ -635,6 +646,10 @@
     @pl.when(jnp.logical_not(last))
     def _():
         rim_copy(me + 1).wait_send()
+
+    @pl.when(me == 0)
+    def _():
+        all_states.wait_recv()
 
     all_scales.wait_send()
     all_segments.wait_send()
@@ -698,7 +713,8 @@
         vmem((1, 2 * heads), F32),
         vmem(conv_taps.shape, BF16),
         vmem((2 * heads, dh), BF16),
-        vmem((slice_rows, dh), F32),
+        vmem((heads, dh, dh), F32),
+        vmem((n_sp, slice_rows, dh), BF16),
         vmem((own, width), BF16),
         vmem((own, width), BF16),
         [half] * 7,

time: 30.7 us -> 30.1 us (0.980)
  Pallas kernels: 30.5 us -> 29.8 us
    pallas_call x1, Pallas kernels: 28.4 us -> 27.7 us  [local_layer(): pl.pallas_call(functools.partial(kernel, n_sp), out_shape=(vmem((own, wid...]
where the time goes in v6:
time: 30.1 us; the launch traced here: 30 us
  Pallas kernels  29.8 us (99%)
    pallas_call x1, Pallas kernels, local_layer(): pl.pallas_call(functools.partial(kernel, n_sp), out_shape=(vmem((own, wid...  27.7 us
    pallas_call x1, Pallas kernels, local_layer(): pl.pallas_call(last_kernel, out_shape=jax.ShapeDtypeStruct(tokens.shape,...  2.11 us

profile of v6, /device:TPU:1, one launch (start us, length us, event | category | flops | bytes accessed | tf_op | source)
XLA Modules:
  0.0 30.0 jit_solution(10100274668425070502)
XLA Ops:
  0.0 27.7 %shard_map.181 = (f32[512,2048]{1,0:T(8,128)S(1)}, bf16[2,256,512]{2,1,0:T(8,128)(2,1)S(1)}, bf16[512,2048]{1,0:T(8,128)(2,1)S(1)}) custom-call(bf16[1,512,2048]{2,1,0:T(8,128)(2,1)} %tokens.1, bf16[16,128]{1,0:T(8,128)(2,1)} %bitcast.10, bf16[2048,512]{1,0:T(8,128)(2,1)} %w_query.1, bf16[2048,512]{1,0:T(8,128)(2,1)} %w_key.1, bf16[2048,512]{1,0:T(8,128)(2,1)} %w_value.1, ...), custom_call_target="tpu_custom_call" | custom-call | tf_op jit(solution)/shard_map/pallas_call | solution.py:751
  27.7 2.1 %shard_map.182 = bf16[1,512,2048]{2,1,0:T(8,128)(2,1)} custom-call(f32[512,2048]{1,0:T(8,128)S(1)} %get-tuple-element.8.acc, bf16[2,256,512]{2,1,0:T(8,128)(2,1)S(1)} %get-tuple-element.9.mem_in, bf16[512,2048]{1,0:T(8,128)(2,1)S(1)} %get-tuple-element.10.wom_in), custom_call_target="tpu_custom_call" | custom-call | tf_op jit(solution)/shard_map/pallas_call | solution.py:771
